TPU v7x, 32 devices: a whole 2x2x4 slice. The times are simulated.
32 devices in a mesh: sp: 8 (over z, x), tp: 4 (over y, core).
Axes of the slice: x: 2, y: 2, z: 4, core: 2. Of those that a mesh axis runs over, the one named last changes fastest.
Arguments:
- tokens: bfloat16 [4096, 2048], P('sp', 'tp'), may hold values from -6 to 6
- norm_gain: float32 [2048], replicated, may hold values from 0.1 to 1.9
- w_query: bfloat16 [2048, 1024], P('sp', 'tp'), may hold values from -1 to 1
- w_key: bfloat16 [2048, 256], P('sp', 'tp'), may hold values from -16 to 16
- w_value: bfloat16 [2048, 256], P('sp', 'tp'), may hold values from -1 to 1
- w_post_gate: bfloat16 [2048, 1024], P('sp', 'tp'), may hold values from -0.125 to 0.125
- w_pre_gate: bfloat16 [2048, 1024], P('sp', 'tp'), may hold values from -0.125 to 0.125
- w_conv_in: bfloat16 [2048, 1024], P('sp', 'tp'), may hold values from -0.125 to 0.125
- conv_taps: float32 [3, 1024], P(None, 'tp'), may hold values from -3 to 3
- sink_logit: float32 [16], P('tp'), may hold values from 2 to 6
- w_out_attn: bfloat16 [1024, 2048], P('tp', 'sp'), may hold values from -0.1875 to 0.1875
- w_out_conv: bfloat16 [1024, 2048], P('tp', 'sp'), may hold values from -0.1875 to 0.1875
Outputs:
- mixed: bfloat16 [4096, 2048], P(('sp', 'tp'))
- log_weight_sum: float32 [16, 4096], P('tp', 'sp')
All inputs are finite; a program needn't handle non-finite values.
Results may differ from a plain program's by a relative error of at most 0.012.
The roundings to bfloat16 on the way count: a program that leaves them out, or rounds other values in their place, can miss the bound.
Values may be sent and summed in bfloat16 or wider, within the bound.
A program may use at most 64 MiB of HBM per device.

v0:
```python
import functools
import math

import jax
import jax.numpy as jnp
from jax import lax
from jax.experimental import pallas as pl
from jax.experimental.pallas import tpu as pltpu
from jax.sharding import PartitionSpec as P

MESH = pl.DeviceIdType.MESH

HEAD_DIM = 64
WINDOW = 128
GRID_W = 64


rope_base = 10000.0
norm_eps = 1e-06


def padded(block, sides, width):
    for axis, dim in sides:
        count = lax.axis_size(axis)
        forward = [(i, i + 1) for i in range(count - 1)]
        backward = [(target, source) for source, target in forward]
        low = lax.ppermute(
            lax.slice_in_dim(block, block.shape[dim] - width, None, axis=dim), axis, forward
        )
        high = lax.ppermute(lax.slice_in_dim(block, 0, width, axis=dim), axis, backward)
        block = jnp.concatenate([low, block, high], axis=dim)
    return block


def rotate_pair(values, angles):
    first_half, second_half = jnp.split(values, 2, axis=-1)
    cosine = jnp.cos(angles)[:, None, :]
    sine_part = jnp.sin(angles)[:, None, :]
    return jnp.concatenate(
        [
            first_half * cosine - second_half * sine_part,
            first_half * sine_part + second_half * cosine,
        ],
        axis=-1,
    )


def axial_rotate(values, positions):
    half_dim = values.shape[-1] // 2
    inv_freq = rope_base ** (-jnp.arange(0, half_dim, 2).astype(jnp.float32) / half_dim)
    row_angle = (positions // GRID_W).astype(jnp.float32)[:, None] * inv_freq
    col_angle = (positions % GRID_W).astype(jnp.float32)[:, None] * inv_freq
    row_part, col_part = jnp.split(values, 2, axis=-1)
    return jnp.concatenate(
        [rotate_pair(row_part, row_angle), rotate_pair(col_part, col_angle)], axis=-1
    )


def block_windows(source, rows_local, blocks):
    pieces = [
        source[step * WINDOW : step * WINDOW + rows_local].reshape(
            (blocks, WINDOW) + source.shape[1:]
        )
        for step in range(3)
    ]
    return jnp.concatenate(pieces, axis=1)


def on_device(
    tokens,
    norm_gain,
    w_query,
    w_key,
    w_value,
    w_post_gate,
    w_pre_gate,
    w_conv_in,
    conv_taps,
    sink_logit,
    w_out_attn,
    w_out_conv,
):
    whole = lax.all_gather(tokens, "tp", axis=1, tiled=True)
    rows_local = whole.shape[0]
    whole_float = whole.astype(jnp.float32)
    mean_square = jnp.mean(whole_float * whole_float, axis=1, keepdims=True)
    normed = (whole_float * lax.rsqrt(mean_square + norm_eps) * norm_gain).astype(jnp.bfloat16)
    col_widths = [
        w_query.shape[1],
        w_key.shape[1],
        w_value.shape[1],
        w_post_gate.shape[1],
        w_pre_gate.shape[1],
        w_conv_in.shape[1],
    ]
    joined = jnp.concatenate(
        (
            lax.all_gather(w_query, "sp", axis=0, tiled=True),
            lax.all_gather(w_key, "sp", axis=0, tiled=True),
            lax.all_gather(w_value, "sp", axis=0, tiled=True),
            lax.all_gather(w_post_gate, "sp", axis=0, tiled=True),
            lax.all_gather(w_pre_gate, "sp", axis=0, tiled=True),
            lax.all_gather(w_conv_in, "sp", axis=0, tiled=True),
        ),
        axis=1,
    )
    projected = jnp.dot(normed, joined, preferred_element_type=jnp.float32)
    bounds = []
    running = 0
    for col_width in col_widths[:-1]:
        running += col_width
        bounds.append(running)
    query_raw, key_raw, value_raw, post_gate, pre_gate, conv_input = jnp.split(
        projected, bounds, axis=1
    )
    offset = lax.axis_index("sp") * rows_local
    positions = offset + jnp.arange(rows_local, dtype=jnp.int32)
    local_heads = w_query.shape[1] // HEAD_DIM
    local_groups = w_key.shape[1] // HEAD_DIM
    group_size = local_heads // local_groups
    queries = axial_rotate(query_raw.reshape(rows_local, local_heads, HEAD_DIM), positions).astype(
        jnp.bfloat16
    )
    keys_rot = axial_rotate(key_raw.reshape(rows_local, local_groups, HEAD_DIM), positions).astype(
        jnp.bfloat16
    )
    key_value = jnp.concatenate(
        [keys_rot.reshape(rows_local, local_groups * HEAD_DIM), value_raw.astype(jnp.bfloat16)],
        axis=1,
    )
    mixed_input = (pre_gate * conv_input).astype(jnp.bfloat16)
    kv_padded = padded(key_value, (("sp", 0),), WINDOW)
    conv_padded = padded(mixed_input, (("sp", 0),), 1)
    conv_float = conv_padded.astype(jnp.float32)
    convolved = (
        conv_taps[0] * conv_float[:-2]
        + conv_taps[1] * conv_float[1:-1]
        + conv_taps[2] * conv_float[2:]
    )
    conv_out = (post_gate * convolved).astype(jnp.bfloat16)
    total_tokens = rows_local * lax.axis_size("sp")
    blocks = rows_local // WINDOW
    padded_rows = rows_local + 2 * WINDOW
    block_queries = queries.reshape(blocks, WINDOW, local_groups, group_size, HEAD_DIM)
    block_keys = block_windows(
        kv_padded[:, : local_groups * HEAD_DIM].reshape(padded_rows, local_groups, HEAD_DIM),
        rows_local,
        blocks,
    )
    block_values = block_windows(
        kv_padded[:, local_groups * HEAD_DIM :].reshape(padded_rows, local_groups, HEAD_DIM),
        rows_local,
        blocks,
    )
    scores = jnp.einsum(
        "nqkgd,nskd->nkgqs", block_queries, block_keys, preferred_element_type=jnp.float32
    ) * HEAD_DIM ** (-0.5)
    query_pos = positions.reshape(blocks, WINDOW)
    key_pos = (
        offset
        - WINDOW
        + (jnp.arange(blocks, dtype=jnp.int32) * WINDOW)[:, None]
        + jnp.arange(3 * WINDOW, dtype=jnp.int32)[None, :]
    )
    distance = key_pos[:, None, :] - query_pos[:, :, None]
    allowed = (
        (jnp.abs(distance) <= WINDOW)
        & (key_pos >= 0)[:, None, :]
        & (key_pos < total_tokens)[:, None, :]
    )
    scores = jnp.where(allowed[:, None, None], scores, -jnp.inf)
    sink_values = sink_logit.reshape(local_groups, group_size)[None, :, :, None]
    row_max = jnp.maximum(jnp.max(scores, axis=-1), sink_values)
    exp_scores = jnp.exp(scores - row_max[..., None])
    denominator = jnp.sum(exp_scores, axis=-1) + jnp.exp(sink_values - row_max)
    weights = (exp_scores / denominator[..., None]).astype(jnp.bfloat16)
    attended = (
        jnp.einsum("nkgqs,nskd->nqkgd", weights, block_values, preferred_element_type=jnp.float32)
        .astype(jnp.bfloat16)
        .reshape(rows_local, local_heads * HEAD_DIM)
    )
    log_sum = row_max + jnp.log(denominator)
    log_weight_sum = jnp.transpose(log_sum, (1, 2, 0, 3)).reshape(local_heads, rows_local)
    out_attn, out_conv = (
        lax.all_gather(w_out_attn, "sp", axis=1, tiled=True),
        lax.all_gather(w_out_conv, "sp", axis=1, tiled=True),
    )
    mixed = lax.psum_scatter(
        (
            jnp.dot(attended, out_attn, preferred_element_type=jnp.float32)
            + jnp.dot(conv_out, out_conv, preferred_element_type=jnp.float32)
        ).astype(jnp.bfloat16),
        "tp",
        scatter_dimension=0,
        tiled=True,
    )
    return (mixed, log_weight_sum)


def fused_kernel(
    Z, X,
    tok_ref, gain_ref, wq_ref, wk_ref, wv_ref, wpost_ref, wpre_ref, wcin_ref, oa_ref, oc_ref, taps_ref, sink_ref,
    out_ref, lse_ref,
    cos_ref, sin_ref, tok, normed, win, woa, woc, acc, qbuf, kvp, cf, chalo_out, chalo_in, att, cout,
    part_keep, part_send, part_recv, y_send, y_recv,
    tok_sem, in_send, in_recv, oa_send, oa_recv, oc_send, oc_recv, halo_sem, rs_sem, loc_sem,
):
    S = Z * X
    rows, width = tok_ref.shape
    depth = wq_ref.shape[0]
    piece = depth // 2
    cols = oa_ref.shape[1]
    qw = qbuf.shape[1]
    cw = cf.shape[1]
    sp = lax.axis_index("sp")
    tp = lax.axis_index("tp")
    z, x = sp // X, sp % X
    core, yy = tp % 2, tp // 2
    sib = tp + 1 - 2 * core
    ynb = (1 - yy) * 2 + core
    ysib = (1 - yy) * 2 + 1 - core
    xnb = z * X + 1 - x
    low, high = sp - X, sp + X
    has_low, has_high = z > 0, z < Z - 1
    has_prev, has_next = sp > 0, sp < S - 1

    kw = 2 * HEAD_DIM
    win[sp, :, 0:qw] = wq_ref[...]
    kv_t = jnp.concatenate([wk_ref[...], wv_ref[...]], axis=0).astype(jnp.float32)
    win[sp, :, qw:qw + kw] = jnp.transpose(kv_t).astype(jnp.bfloat16)
    for part, ref in enumerate((wpost_ref, wpre_ref, wcin_ref)):
        win[sp, :, qw + kw + part * cw:qw + kw + (part + 1) * cw] = ref[...]

    barrier = pltpu.get_barrier_semaphore()

    def greet(dev):
        pl.semaphore_signal(barrier, inc=1, device_id=dev, device_id_type=MESH)

    greet((xnb, tp))
    greet((sp, sib))
    greet((sp, ynb))
    for cond, dev in ((has_low, low), (has_high, high), (has_prev, sp - 1), (has_next, sp + 1)):
        @pl.when(cond)
        def _(dev=dev):
            greet((dev, tp))
    peers = 3
    for cond in (has_low, has_high, has_prev, has_next):
        peers = peers + jnp.where(cond, 1, 0)
    pl.semaphore_wait(barrier, peers)

    def remote(src, dst, ssem, rsem, dev):
        return pltpu.make_async_remote_copy(
            src_ref=src, dst_ref=dst, send_sem=ssem, recv_sem=rsem,
            device_id=dev, device_id_type=MESH,
        )

    targets = (low, high, xnb)

    def in_copy(slot, half, direction):
        block = win.at[slot, pl.ds(half * piece, piece)]
        return remote(
            block, block, in_send.at[direction, half, slot], in_recv.at[half, slot], (targets[direction], tp)
        )

    def weight_copy(kind, slot, direction, own=False):
        buf, ssem, rsem, ref = ((woa, oa_send, oa_recv, oa_ref), (woc, oc_send, oc_recv, oc_ref))[kind - 1]
        source = ref if own else buf.at[slot]
        return remote(source, buf.at[slot], ssem.at[direction, slot], rsem.at[slot], (targets[direction], tp))

    weight_copy(2, sp, 2, True).start()
    for half in range(2):
        for direction, cond in ((0, has_low), (1, has_high)):
            @pl.when(cond)
            def _(half=half, direction=direction):
                in_copy(sp, half, direction).start()
        in_copy(sp, half, 2).start()

    tok_y = remote(tok_ref, tok.at[tp], tok_sem.at[0], tok_sem.at[1], (sp, ynb))
    tok_y.start()
    tok_s = remote(tok_ref, tok.at[tp], tok_sem.at[2], tok_sem.at[3], (sp, sib))
    tok_s.start()
    local = [
        pltpu.make_async_copy(tok_ref, tok.at[tp], loc_sem.at[0]),
        pltpu.make_async_copy(oa_ref, woa.at[sp], loc_sem.at[2]),
        pltpu.make_async_copy(oc_ref, woc.at[sp], loc_sem.at[3]),
    ]
    for copy in local:
        copy.start()

    MB = 128
    quarter = HEAD_DIM // 4

    def angles(i, carry):
        r = pl.ds(pl.multiple_of(i * MB, MB), MB)
        pos = sp * rows + i * MB + lax.broadcasted_iota(jnp.int32, (MB, kw), 0)
        lane = lax.broadcasted_iota(jnp.int32, (MB, kw), 1) % HEAD_DIM
        freq = jnp.exp((lane % quarter).astype(jnp.float32) * (-4.0 / HEAD_DIM * math.log(rope_base)))
        index = jnp.where(lane >= 2 * quarter, pos % GRID_W, pos // GRID_W)
        angle = index.astype(jnp.float32) * freq
        cos_ref[r, :] = jnp.cos(angle)
        sin_ref[r, :] = jnp.where(lane % (2 * quarter) < quarter, -1.0, 1.0) * jnp.sin(angle)
        return carry

    lax.fori_loop(0, rows // MB, angles, 0)

    def in_comm(dist):
        for half in range(2):
            for up in (0, 1):
                zz = z + dist * (2 * up - 1)

                @pl.when((zz >= 0) & (zz < Z))
                def _(zz=zz, half=half, up=up):
                    slot = zz * X + x
                    in_copy(slot, half, 2).wait_recv()
                    @pl.when(has_low if up else has_high)
                    def _():
                        in_copy(slot, half, 0 if up else 1).start()
                    in_copy(slot, half, 2).start()

    in_comm(1)
    for copy in local:
        copy.wait()
    remote(tok.at[ynb], tok.at[ynb], tok_sem.at[0], tok_sem.at[1], (sp, ynb)).wait_recv()
    tok_f = remote(tok.at[ynb], tok.at[ynb], tok_sem.at[4], tok_sem.at[5], (sp, sib))
    tok_f.start()
    remote(tok.at[sib], tok.at[sib], tok_sem.at[2], tok_sem.at[3], (sp, sib)).wait_recv()
    remote(tok.at[ysib], tok.at[ysib], tok_sem.at[4], tok_sem.at[5], (sp, sib)).wait_recv()

    TP = tok.shape[0]
    RB = 64

    def norm_rows(i, carry):
        r = pl.ds(pl.multiple_of(i * RB, RB), RB)
        total = jnp.zeros((RB, 1), jnp.float32)
        for t in range(TP):
            v = tok[t, r, :].astype(jnp.float32)
            total += jnp.sum(v * v, axis=1, keepdims=True)
        scale = lax.rsqrt(total / (TP * width) + norm_eps)
        for t in range(TP):
            v = tok[t, r, :].astype(jnp.float32)
            g = gain_ref[:, t * width:(t + 1) * width]
            normed[r, t * width:(t + 1) * width] = (v * scale * g).astype(jnp.bfloat16)
        return carry

    lax.fori_loop(0, rows // RB, norm_rows, 0)

    def project(slot, first):
        def body(i, carry):
            r = pl.ds(pl.multiple_of(i * MB, MB), MB)
            c = pl.ds(pl.multiple_of(slot * depth, depth), depth)
            prod = jnp.dot(normed[r, c], win[slot], preferred_element_type=jnp.float32)
            if first:
                acc[r, :] = prod
            else:
                acc[r, :] += prod
            return carry
        lax.fori_loop(0, rows // MB, body, 0)

    def entry(k):
        dist = (k + 1) // 2
        up = 1 - k % 2
        zz = z + dist * (2 * up - 1)
        return zz, up, (zz >= 0) & (zz < Z)

    def wait_weight(kind, slot):
        weight_copy(kind, slot, 2).wait_recv()

    def pass_on(kind, slot, up, across):
        @pl.when((up == 1) & has_low)
        def _():
            weight_copy(kind, slot, 0).start()
        @pl.when((up == 0) & has_high)
        def _():
            weight_copy(kind, slot, 1).start()
        if across:
            weight_copy(kind, slot, 2).start()

    entries = 2 * Z - 1

    def start_out_weights():
        for direction, cond in ((0, has_low), (1, has_high)):
            @pl.when(cond)
            def _(direction=direction):
                weight_copy(1, sp, direction, True).start()
                weight_copy(2, sp, direction, True).start()
        weight_copy(1, sp, 2, True).start()
        wait_weight(2, xnb)
        for direction, cond in ((0, has_low), (1, has_high)):
            @pl.when(cond)
            def _(direction=direction):
                weight_copy(2, xnb, direction).start()

    project(sp, True)

    def out_comm(dist):
        for kind, across, far in ((1, True, False), (2, False, False), (2, False, True)):
            for up in (0, 1):
                zz = z + dist * (2 * up - 1)

                @pl.when((zz >= 0) & (zz < Z))
                def _(zz=zz, up=up, kind=kind, across=across, far=far):
                    slot = zz * X + (1 - x if far else x)
                    wait_weight(kind, slot)
                    pass_on(kind, slot, up, across)

    def in_step(dist, carry):
        @pl.when(dist > 1)
        def _():
            in_comm(dist)

        @pl.when(dist == Z - 2)
        def _():
            start_out_weights()

        @pl.when(dist == Z - 1)
        def _():
            out_comm(1)

        def work(side, carry):
            zz = z + dist * (2 * side - 1)

            @pl.when((zz >= 0) & (zz < Z))
            def _():
                project(zz * X + x, False)
            zo = z + (dist - 1) * (2 * side - 1)

            @pl.when((zo >= 0) & (zo < Z) & ((dist > 1) | (side == 0)))
            def _():
                slot = zo * X + 1 - x
                for half in range(2):
                    in_copy(slot, half, 2).wait_recv()
                project(slot, False)
            return carry

        lax.fori_loop(0, 2, work, 0)
        return carry

    lax.fori_loop(1, Z + 1, in_step, 0)

    def turned(v, cosv, sinv):
        lane = lax.broadcasted_iota(jnp.int32, v.shape, 1)
        partner = jnp.where(
            lane % (2 * quarter) < quarter,
            pltpu.roll(v, v.shape[1] - quarter, 1),
            pltpu.roll(v, quarter, 1),
        )
        return v * cosv + partner * sinv

    def kv_rows(i, carry):
        r = pl.ds(pl.multiple_of(i * MB, MB), MB)
        v = acc[r, qw:qw + kw]
        lane = lax.broadcasted_iota(jnp.int32, v.shape, 1)
        kv = jnp.where(lane < HEAD_DIM, turned(v, cos_ref[r, :], sin_ref[r, :]), v)
        kvp[pl.ds(pl.multiple_of(WINDOW + i * MB, MB), MB), :] = kv.astype(jnp.bfloat16)
        base = qw + kw + cw
        mi = (acc[r, base:base + cw] * acc[r, base + cw:base + 2 * cw]).astype(jnp.bfloat16)
        cf[pl.ds(pl.multiple_of(8 + i * MB, 8), MB), :] = mi.astype(jnp.float32)
        return carry

    lax.fori_loop(0, rows // MB, kv_rows, 0)
    E = chalo_out.shape[1]
    chalo_out[0] = cf[8:8 + E, :].astype(jnp.bfloat16)
    chalo_out[1] = cf[8 + rows - E:8 + rows, :].astype(jnp.bfloat16)

    to_next = [
        remote(kvp.at[pl.ds(rows, WINDOW)], kvp.at[pl.ds(0, WINDOW)], halo_sem.at[0], halo_sem.at[1], (sp + 1, tp)),
        remote(chalo_out.at[1], chalo_in.at[0], halo_sem.at[2], halo_sem.at[3], (sp + 1, tp)),
    ]
    to_prev = [
        remote(kvp.at[pl.ds(WINDOW, WINDOW)], kvp.at[pl.ds(WINDOW + rows, WINDOW)], halo_sem.at[4], halo_sem.at[5], (sp - 1, tp)),
        remote(chalo_out.at[0], chalo_in.at[1], halo_sem.at[6], halo_sem.at[7], (sp - 1, tp)),
    ]

    @pl.when(has_next)
    def _():
        for copy in to_next:
            copy.start()

    @pl.when(has_prev)
    def _():
        for copy in to_prev:
            copy.start()

    if Z > 2:
        out_comm(2)

    def q_rows(i, carry):
        r = pl.ds(pl.multiple_of(i * MB, MB), MB)
        for c in range(qw // kw):
            qbuf[r, c * kw:(c + 1) * kw] = turned(
                acc[r, c * kw:(c + 1) * kw], cos_ref[r, :], sin_ref[r, :]
            ).astype(jnp.bfloat16)
        return carry

    lax.fori_loop(0, rows // MB, q_rows, 0)

    zero_kv = jnp.zeros((WINDOW, kw), jnp.bfloat16)
    zero_c = jnp.zeros((8, cw), jnp.float32)

    @pl.when(has_prev)
    def _():
        for copy in to_next:
            copy.wait_recv()
        cf[0:8, :] = chalo_in[0, E - 8:E, :].astype(jnp.float32)

    @pl.when(jnp.logical_not(has_prev))
    def _():
        kvp[0:WINDOW, :] = zero_kv
        cf[0:8, :] = zero_c

    @pl.when(has_next)
    def _():
        for copy in to_prev:
            copy.wait_recv()
        cf[8 + rows:16 + rows, :] = chalo_in[1, 0:8, :].astype(jnp.float32)

    @pl.when(jnp.logical_not(has_next))
    def _():
        kvp[WINDOW + rows:, :] = zero_kv
        cf[8 + rows:16 + rows, :] = zero_c

    taps = [taps_ref[t:t + 1, :] for t in range(3)]
    for i in range(rows // MB):
        a = 8 + i * MB
        conv = (
            taps[0] * cf[a - 1:a - 1 + MB, :]
            + taps[1] * cf[a:a + MB, :]
            + taps[2] * cf[a + 1:a + 1 + MB, :]
        )
        cout[i * MB:(i + 1) * MB, :] = (acc[i * MB:(i + 1) * MB, qw + kw:qw + kw + cw] * conv).astype(jnp.bfloat16)

    heads = qw // HEAD_DIM
    K3 = 3 * WINDOW
    total_tokens = rows * S

    def attend(b, carry):
        r = pl.ds(pl.multiple_of(b * WINDOW, WINDOW), WINDOW)
        kv = kvp[pl.ds(pl.multiple_of(b * WINDOW, WINDOW), K3), :].astype(jnp.float32)
        lane = lax.broadcasted_iota(jnp.int32, (K3, kw), 1)
        swapped = pltpu.roll(kv, HEAD_DIM, 1)
        kk = jnp.where(lane < HEAD_DIM, kv, swapped).astype(jnp.bfloat16)
        vv = jnp.where(lane < HEAD_DIM, swapped, kv).astype(jnp.bfloat16)
        k_half = [jnp.where(lane < HEAD_DIM, kk, 0), jnp.where(lane < HEAD_DIM, 0, kk)]
        v_half = [jnp.where(lane < HEAD_DIM, vv, 0), jnp.where(lane < HEAD_DIM, 0, vv)]
        qi = lax.broadcasted_iota(jnp.int32, (WINDOW, K3), 0)
        ki = lax.broadcasted_iota(jnp.int32, (WINDOW, K3), 1)
        first = sp * rows + b * WINDOW - WINDOW
        allowed = (ki >= qi) & (ki <= qi + 2 * WINDOW) & (ki + first >= 0) & (ki + first < total_tokens)
        lse_lane = lax.broadcasted_iota(jnp.int32, (WINDOW, WINDOW), 1)
        lse_all = jnp.zeros((WINDOW, WINDOW), jnp.float32)
        for pair in range(heads // 2):
            q = qbuf[r, pair * kw:(pair + 1) * kw]
            total = jnp.zeros((WINDOW, kw), jnp.float32)
            for side in range(2):
                h = pair * 2 + side
                s = lax.dot_general(
                    q, k_half[side], (((1,), (1,)), ((), ())), preferred_element_type=jnp.float32
                ) * HEAD_DIM ** (-0.5)
                s = jnp.where(allowed, s, -jnp.inf)
                sink = sink_ref[h]
                top = jnp.maximum(jnp.max(s, axis=1, keepdims=True), sink)
                e = jnp.exp(s - top)
                den = jnp.sum(e, axis=1, keepdims=True) + jnp.exp(sink - top)
                w = (e * (1.0 / den)).astype(jnp.bfloat16)
                total += jnp.dot(w, v_half[side], preferred_element_type=jnp.float32)
                lse_all = jnp.where(lse_lane == h, top + jnp.log(den), lse_all)
            att[r, pair * kw:(pair + 1) * kw] = total.astype(jnp.bfloat16)
        lse_ref[:, r] = jnp.transpose(lse_all)[0:heads, :]
        return carry

    blocks = rows // WINDOW
    lax.fori_loop(0, blocks, attend, 0)

    chunk = rows // TP

    def sib_copy(slot):
        return remote(part_send.at[slot], part_recv.at[slot], rs_sem.at[0, slot], rs_sem.at[1, slot], (sp, sib))

    def y_copy(slot):
        return remote(y_send.at[slot], y_recv.at[slot], rs_sem.at[2, slot], rs_sem.at[3, slot], (sp, ynb))

    def out_block(slot):
        for half in range(2):
            for mine in range(2):
                t = half * 2 + (core if mine else 1 - core)
                r = pl.ds(pl.multiple_of(t * chunk, chunk), chunk)
                v = jnp.dot(att[r, :], woa[slot], preferred_element_type=jnp.float32) + jnp.dot(
                    cout[r, :], woc[slot], preferred_element_type=jnp.float32
                )
                if mine:
                    part_keep[slot, half] = v
                else:
                    part_send[slot, half] = v.astype(jnp.bfloat16)
        sib_copy(slot).start()

    def y_block(slot):
        sib_copy(slot).wait_recv()
        y_send[slot] = (
            part_keep[slot, 1 - yy] + part_recv[slot, 1 - yy].astype(jnp.float32)
        ).astype(jnp.bfloat16)
        y_copy(slot).start()

    def finish(slot):
        y_copy(slot).wait_recv()
        out_ref[:, pl.ds(pl.multiple_of(slot * cols, cols), cols)] = (
            part_keep[slot, yy]
            + part_recv[slot, yy].astype(jnp.float32)
            + y_recv[slot].astype(jnp.float32)
        ).astype(jnp.bfloat16)

    def each(fn, lo, hi):
        def step(u, carry):
            k, side = u // 2, u % 2
            zz, _, valid = entry(k)

            @pl.when(valid)
            def _():
                slot = zz * X + jnp.where(side == 0, x, 1 - x)
                fn(slot, k, side)
            return carry
        lax.fori_loop(lo, hi, step, 0)

    def project_out(slot, k, side):
        @pl.when(side == 1)
        def _():
            wait_weight(1, slot)
        out_block(slot)

    early = min(6, 2 * entries)
    each(project_out, 0, early)
    each(lambda slot, k, side: y_block(slot), 0, early)
    for dist in range(2, Z):
        if dist > 2:
            out_comm(dist)
        lo, hi = 4 * dist - 2, 4 * dist + 2
        each(project_out, lo, hi)
        each(lambda slot, k, side: y_block(slot), lo, hi)
    each(lambda slot, k, side: finish(slot), 0, 2 * entries)

    tok_y.wait_send()
    tok_s.wait_send()
    tok_f.wait_send()

    @pl.when(has_next)
    def _():
        for copy in to_next:
            copy.wait_send()

    @pl.when(has_prev)
    def _():
        for copy in to_prev:
            copy.wait_send()

    def drain(zz, carry):
        mine, other = zz * X + x, zz * X + 1 - x
        for direction, cond in ((0, (zz >= z) & has_low), (1, (zz <= z) & has_high)):
            @pl.when(cond)
            def _(direction=direction):
                in_copy(mine, 0, direction).wait_send()
                in_copy(mine, 1, direction).wait_send()
                weight_copy(1, mine, direction).wait_send()
                weight_copy(2, mine, direction).wait_send()
                weight_copy(2, other, direction).wait_send()
        in_copy(mine, 0, 2).wait_send()
        in_copy(mine, 1, 2).wait_send()
        weight_copy(1, mine, 2).wait_send()
        for slot in (mine, other):
            sib_copy(slot).wait_send()
            y_copy(slot).wait_send()
        return carry

    lax.fori_loop(0, Z, drain, 0)
    weight_copy(2, sp, 2).wait_send()


def fused(
    tokens, norm_gain, w_query, w_key, w_value, w_post_gate, w_pre_gate, w_conv_in,
    conv_taps, sink_logit, w_out_attn, w_out_conv,
):
    S, TP = lax.axis_size("sp"), lax.axis_size("tp")
    X = 2
    Z = S // X
    rows, width = tokens.shape
    depth, qw = w_query.shape
    cw = w_post_gate.shape[1]
    cols = w_out_attn.shape[1]
    heads = qw // HEAD_DIM
    kw = 2 * HEAD_DIM
    nw = qw + kw + 3 * cw
    chunk = rows // TP
    bf, f32 = jnp.bfloat16, jnp.float32
    dma = pltpu.SemaphoreType.DMA
    return pl.pallas_call(
        functools.partial(fused_kernel, Z, X),
        out_shape=(
            jax.ShapeDtypeStruct((chunk, S * cols), bf),
            jax.ShapeDtypeStruct((heads, rows), f32),
        ),
        in_specs=[pl.BlockSpec(memory_space=pltpu.VMEM)] * 11 + [pl.BlockSpec(memory_space=pltpu.SMEM)],
        out_specs=(pl.BlockSpec(memory_space=pltpu.VMEM),) * 2,
        scratch_shapes=[
            pltpu.VMEM((rows, kw), f32),
            pltpu.VMEM((rows, kw), f32),
            pltpu.VMEM((TP, rows, width), bf),
            pltpu.VMEM((rows, TP * width), bf),
            pltpu.VMEM((S, depth, nw), bf),
            pltpu.VMEM((S,) + w_out_attn.shape, bf),
            pltpu.VMEM((S,) + w_out_conv.shape, bf),
            pltpu.VMEM((rows, nw), f32),
            pltpu.VMEM((rows, qw), bf),
            pltpu.VMEM((rows + 2 * WINDOW, kw), bf),
            pltpu.VMEM((rows + 16, cw), f32),
            pltpu.VMEM((2, 16, cw), bf),
            pltpu.VMEM((2, 16, cw), bf),
            pltpu.VMEM((rows, qw), bf),
            pltpu.VMEM((rows, cw), bf),
            pltpu.VMEM((S, 2, chunk, cols), f32),
            pltpu.VMEM((S, 2, chunk, cols), bf),
            pltpu.VMEM((S, 2, chunk, cols), bf),
            pltpu.VMEM((S, chunk, cols), bf),
            pltpu.VMEM((S, chunk, cols), bf),
            dma((6,)),
            dma((3, 2, S)), dma((2, S)),
            dma((3, S)), dma((S,)),
            dma((3, S)), dma((S,)),
            dma((8,)),
            dma((4, S)),
            dma((4,)),
        ],
        compiler_params=pltpu.CompilerParams(
            collective_id=0, has_side_effects=True, vmem_limit_bytes=60 * 1024 * 1024
        ),
    )(
        tokens, norm_gain[None, :], w_query, w_key.T, w_value.T, w_post_gate, w_pre_gate, w_conv_in,
        w_out_attn, w_out_conv, conv_taps, sink_logit,
    )


def fits(
    tokens, norm_gain, w_query, w_key, w_value, w_post_gate, w_pre_gate, w_conv_in,
    conv_taps, sink_logit, w_out_attn, w_out_conv,
):
    S, TP = lax.axis_size("sp"), lax.axis_size("tp")
    return (
        TP == 4
        and S % 2 == 0
        and S >= 6
        and w_key.shape[1] == HEAD_DIM
        and w_query.shape[0] % 128 == 0
        and w_query.shape[1] % 128 == 0
        and w_post_gate.shape[1] % 128 == 0
        and w_out_attn.shape[1] % 128 == 0
        and tokens.shape[0] % (TP * WINDOW) == 0
        and tokens.shape[1] % 128 == 0
    )


def either(*args):
    return fused(*args) if fits(*args) else on_device(*args)


def solution(mesh):
    placed = (
        P("sp", "tp"),
        P(),
        P("sp", "tp"),
        P("sp", "tp"),
        P("sp", "tp"),
        P("sp", "tp"),
        P("sp", "tp"),
        P("sp", "tp"),
        P(None, "tp"),
        P("tp"),
        P("tp", "sp"),
        P("tp", "sp"),
    )
    return jax.shard_map(
        either,
        mesh=mesh,
        in_specs=placed,
        out_specs=(P(("sp", "tp"), None), P("tp", "sp")),
        check_vma=False,
    )
```

profile of v0, /device:TPU:16, one launch (start us, length us, event | category | flops | bytes accessed | tf_op | source)
XLA Modules:
  0.0 95.5 jit_solution(13633581503702134390)
XLA Ops:
  0.6 92.4 %shard_map.131 = (bf16[128,2048]{1,0:T(8,128)(2,1)}, f32[4,512]{1,0:T(4,128)}) custom-call(bf16[512,512]{1,0:T(8,128)(2,1)} %tok_ref.1, f32[1,2048]{1,0:T(1,128)} %bitcast.5, bf16[256,256]{1,0:T(8,128)(2,1)} %wq_ref.1, bf16[64,256]{1,0:T(8,128)(2,1)} %bitcast.3, bf16[64,256]{1,0:T(8,128)(2,1)} %bitcast.4, bf16[256,256]{1,0:T(8,128)(2,1)} %wpost_ref.1, ...), custom_call_target="tpu_custom_call" | custom-call | tf_op jit(solution)/shard_map/pallas_call | solution.py:693
  93.0 0.0 copy-start
  93.0 1.9 %copy.16 = bf16[128,2048]{1,0:T(8,128)(2,1)} copy(bf16[128,2048]{1,0:T(8,128)(2,1)} %get-tuple-element.4) | data formatting | bytes 1048576
  94.9 0.0 copy-done
  94.9 0.6 copy.17
Async XLA Ops:
  93.0 1.9 %copy-start = (f32[4,512]{1,0:T(4,128)S(1)}, f32[4,512]{1,0:T(4,128)}, u32[]{:S(2)}) copy-start(f32[4,512]{1,0:T(4,128)} %get-tuple-element.5) | copy-start | bytes 24580
where the time goes:
time: 95.7 us; the launch traced here: 95.5 us
  Pallas kernels  92.4 us (97%)
  local copies, waits for them, and re-layouts  2.49 us (3%)
    pallas_call x1, Pallas kernels, fused(): pl.pallas_call(functools.partial(fused_kernel, Z, X), out_shape=(jax.Shap...  92.4 us
    unnamed x4, local copies, waits for them, and re-layouts  2.49 us

commit v1 on v0

v1 whole, which is shorter than its diff:
```python
import functools
import math

import jax
import jax.numpy as jnp
from jax import lax
from jax.experimental import pallas as pl
from jax.experimental.pallas import tpu as pltpu
from jax.sharding import PartitionSpec as P

MESH = pl.DeviceIdType.MESH

HEAD_DIM = 64
WINDOW = 128
GRID_W = 64


rope_base = 10000.0
norm_eps = 1e-06


def padded(block, sides, width):
    for axis, dim in sides:
        count = lax.axis_size(axis)
        forward = [(i, i + 1) for i in range(count - 1)]
        backward = [(target, source) for source, target in forward]
        low = lax.ppermute(
            lax.slice_in_dim(block, block.shape[dim] - width, None, axis=dim), axis, forward
        )
        high = lax.ppermute(lax.slice_in_dim(block, 0, width, axis=dim), axis, backward)
        block = jnp.concatenate([low, block, high], axis=dim)
    return block


def rotate_pair(values, angles):
    first_half, second_half = jnp.split(values, 2, axis=-1)
    cosine = jnp.cos(angles)[:, None, :]
    sine_part = jnp.sin(angles)[:, None, :]
    return jnp.concatenate(
        [
            first_half * cosine - second_half * sine_part,
            first_half * sine_part + second_half * cosine,
        ],
        axis=-1,
    )


def axial_rotate(values, positions):
    half_dim = values.shape[-1] // 2
    inv_freq = rope_base ** (-jnp.arange(0, half_dim, 2).astype(jnp.float32) / half_dim)
    row_angle = (positions // GRID_W).astype(jnp.float32)[:, None] * inv_freq
    col_angle = (positions % GRID_W).astype(jnp.float32)[:, None] * inv_freq
    row_part, col_part = jnp.split(values, 2, axis=-1)
    return jnp.concatenate(
        [rotate_pair(row_part, row_angle), rotate_pair(col_part, col_angle)], axis=-1
    )


def block_windows(source, rows_local, blocks):
    pieces = [
        source[step * WINDOW : step * WINDOW + rows_local].reshape(
            (blocks, WINDOW) + source.shape[1:]
        )
        for step in range(3)
    ]
    return jnp.concatenate(pieces, axis=1)


def on_device(
    tokens,
    norm_gain,
    w_query,
    w_key,
    w_value,
    w_post_gate,
    w_pre_gate,
    w_conv_in,
    conv_taps,
    sink_logit,
    w_out_attn,
    w_out_conv,
):
    whole = lax.all_gather(tokens, "tp", axis=1, tiled=True)
    rows_local = whole.shape[0]
    whole_float = whole.astype(jnp.float32)
    mean_square = jnp.mean(whole_float * whole_float, axis=1, keepdims=True)
    normed = (whole_float * lax.rsqrt(mean_square + norm_eps) * norm_gain).astype(jnp.bfloat16)
    col_widths = [
        w_query.shape[1],
        w_key.shape[1],
        w_value.shape[1],
        w_post_gate.shape[1],
        w_pre_gate.shape[1],
        w_conv_in.shape[1],
    ]
    joined = jnp.concatenate(
        (
            lax.all_gather(w_query, "sp", axis=0, tiled=True),
            lax.all_gather(w_key, "sp", axis=0, tiled=True),
            lax.all_gather(w_value, "sp", axis=0, tiled=True),
            lax.all_gather(w_post_gate, "sp", axis=0, tiled=True),
            lax.all_gather(w_pre_gate, "sp", axis=0, tiled=True),
            lax.all_gather(w_conv_in, "sp", axis=0, tiled=True),
        ),
        axis=1,
    )
    projected = jnp.dot(normed, joined, preferred_element_type=jnp.float32)
    bounds = []
    running = 0
    for col_width in col_widths[:-1]:
        running += col_width
        bounds.append(running)
    query_raw, key_raw, value_raw, post_gate, pre_gate, conv_input = jnp.split(
        projected, bounds, axis=1
    )
    offset = lax.axis_index("sp") * rows_local
    positions = offset + jnp.arange(rows_local, dtype=jnp.int32)
    local_heads = w_query.shape[1] // HEAD_DIM
    local_groups = w_key.shape[1] // HEAD_DIM
    group_size = local_heads // local_groups
    queries = axial_rotate(query_raw.reshape(rows_local, local_heads, HEAD_DIM), positions).astype(
        jnp.bfloat16
    )
    keys_rot = axial_rotate(key_raw.reshape(rows_local, local_groups, HEAD_DIM), positions).astype(
        jnp.bfloat16
    )
    key_value = jnp.concatenate(
        [keys_rot.reshape(rows_local, local_groups * HEAD_DIM), value_raw.astype(jnp.bfloat16)],
        axis=1,
    )
    mixed_input = (pre_gate * conv_input).astype(jnp.bfloat16)
    kv_padded = padded(key_value, (("sp", 0),), WINDOW)
    conv_padded = padded(mixed_input, (("sp", 0),), 1)
    conv_float = conv_padded.astype(jnp.float32)
    convolved = (
        conv_taps[0] * conv_float[:-2]
        + conv_taps[1] * conv_float[1:-1]
        + conv_taps[2] * conv_float[2:]
    )
    conv_out = (post_gate * convolved).astype(jnp.bfloat16)
    total_tokens = rows_local * lax.axis_size("sp")
    blocks = rows_local // WINDOW
    padded_rows = rows_local + 2 * WINDOW
    block_queries = queries.reshape(blocks, WINDOW, local_groups, group_size, HEAD_DIM)
    block_keys = block_windows(
        kv_padded[:, : local_groups * HEAD_DIM].reshape(padded_rows, local_groups, HEAD_DIM),
        rows_local,
        blocks,
    )
    block_values = block_windows(
        kv_padded[:, local_groups * HEAD_DIM :].reshape(padded_rows, local_groups, HEAD_DIM),
        rows_local,
        blocks,
    )
    scores = jnp.einsum(
        "nqkgd,nskd->nkgqs", block_queries, block_keys, preferred_element_type=jnp.float32
    ) * HEAD_DIM ** (-0.5)
    query_pos = positions.reshape(blocks, WINDOW)
    key_pos = (
        offset
        - WINDOW
        + (jnp.arange(blocks, dtype=jnp.int32) * WINDOW)[:, None]
        + jnp.arange(3 * WINDOW, dtype=jnp.int32)[None, :]
    )
    distance = key_pos[:, None, :] - query_pos[:, :, None]
    allowed = (
        (jnp.abs(distance) <= WINDOW)
        & (key_pos >= 0)[:, None, :]
        & (key_pos < total_tokens)[:, None, :]
    )
    scores = jnp.where(allowed[:, None, None], scores, -jnp.inf)
    sink_values = sink_logit.reshape(local_groups, group_size)[None, :, :, None]
    row_max = jnp.maximum(jnp.max(scores, axis=-1), sink_values)
    exp_scores = jnp.exp(scores - row_max[..., None])
    denominator = jnp.sum(exp_scores, axis=-1) + jnp.exp(sink_values - row_max)
    weights = (exp_scores / denominator[..., None]).astype(jnp.bfloat16)
    attended = (
        jnp.einsum("nkgqs,nskd->nqkgd", weights, block_values, preferred_element_type=jnp.float32)
        .astype(jnp.bfloat16)
        .reshape(rows_local, local_heads * HEAD_DIM)
    )
    log_sum = row_max + jnp.log(denominator)
    log_weight_sum = jnp.transpose(log_sum, (1, 2, 0, 3)).reshape(local_heads, rows_local)
    out_attn, out_conv = (
        lax.all_gather(w_out_attn, "sp", axis=1, tiled=True),
        lax.all_gather(w_out_conv, "sp", axis=1, tiled=True),
    )
    mixed = lax.psum_scatter(
        (
            jnp.dot(attended, out_attn, preferred_element_type=jnp.float32)
            + jnp.dot(conv_out, out_conv, preferred_element_type=jnp.float32)
        ).astype(jnp.bfloat16),
        "tp",
        scatter_dimension=0,
        tiled=True,
    )
    return (mixed, log_weight_sum)


def fused_kernel(
    Z, X,
    tok_ref, gain_ref, wq_ref, wk_ref, wv_ref, wpost_ref, wpre_ref, wcin_ref, oa_ref, oc_ref, taps_ref, sink_ref,
    out_ref, lse_ref,
    cos_ref, sin_ref, tok, normed, win_a, win_b, wo, acc_a, acc_b, qbuf, kvp, cf, chalo_out, chalo_in, ac, ext, lse_buf,
    keep, send1, recv1, send2, recv2,
    tok_send, tok_recv, w_send, w_recv, sw_send, sw_recv, halo_sem, r1_send, r1_recv, r2_send, r2_recv, loc_sem,
):
    S = Z * X
    rows, width = tok_ref.shape
    depth = wq_ref.shape[0]
    ow, cols = oa_ref.shape
    qw = qbuf.shape[1]
    cw = cf.shape[1]
    kw = 2 * HEAD_DIM
    TP = tok.shape[0]
    chunk = rows // TP
    sp = lax.axis_index("sp")
    tp = lax.axis_index("tp")
    z, x = sp // X, sp % X
    c, y = tp % 2, tp // 2
    vs = z * X + c
    home, foreign = c == x, c != x
    role = jnp.where(home, 0, 1)
    sib = (sp, y * 2 + 1 - c)
    ynb = (sp, (1 - y) * 2 + c)
    yoth = (sp, (1 - y) * 2 + 1 - c)
    xnb = (z * X + 1 - x, tp)
    swp = (z * X + 1 - x, y * 2 + 1 - c)
    low, high = (sp - X, tp), (sp + X, tp)
    has_low, has_high = z > 0, z < Z - 1
    has_prev, has_next = vs > 0, vs < S - 1
    vn, vp = vs + 1, vs - 1 + S
    next_dev = ((vn // X) * X + x, y * 2 + vn % X)
    prev_dev = ((vp // X - Z) * X + x, y * 2 + vp % X)

    barrier = pltpu.get_barrier_semaphore()

    def greet(dev):
        pl.semaphore_signal(barrier, inc=1, device_id=dev, device_id_type=MESH)

    for dev in (sib, ynb, yoth, xnb, swp):
        greet(dev)
    peers = 5
    across_z = ((has_low, low), (has_high, high), (has_prev & (c == 0), prev_dev), (has_next & (c == 1), next_dev))
    for cond, dev in across_z:
        @pl.when(cond)
        def _(dev=dev):
            greet(dev)
        peers = peers + jnp.where(cond, 1, 0)

    pslot = jnp.where(home, sp, S)
    win_a[pslot, :, 0:qw] = wq_ref[...]
    kv_t = jnp.concatenate([wk_ref[...], wv_ref[...]], axis=0).astype(jnp.float32)
    win_a[pslot, :, qw:qw + kw] = jnp.transpose(kv_t).astype(jnp.bfloat16)
    for part, ref in enumerate((wpost_ref, wpre_ref, wcin_ref)):
        win_b[pslot, :, part * cw:(part + 1) * cw] = ref[...]
    heads = qw // HEAD_DIM
    ext[0] = jnp.zeros(ext.shape[1:], jnp.float32)
    ext[0, 0:3, :] = taps_ref[...]
    ext_lane = lax.broadcasted_iota(jnp.int32, (1, cw), 1)
    sink_row = jnp.zeros((1, cw), jnp.float32)
    for h in range(heads):
        sink_row = jnp.where(ext_lane == h, sink_ref[h], sink_row)
    ext[0, 3:4, :] = sink_row

    pl.semaphore_wait(barrier, peers)

    def remote(src, dst, ssem, rsem, dev):
        return pltpu.make_async_remote_copy(
            src_ref=src, dst_ref=dst, send_sem=ssem, recv_sem=rsem,
            device_id=dev, device_id_type=MESH,
        )

    bufs = (win_a, win_b, wo)
    targets = (low, high, sib)

    def wcopy(kind, slot, direction):
        block = bufs[kind].at[slot]
        return remote(block, block, w_send.at[kind, direction, slot], w_recv.at[kind, slot], targets[direction])

    def own_start(kind):
        for direction, cond in ((0, has_low), (1, has_high)):
            @pl.when(cond)
            def _(direction=direction):
                wcopy(kind, vs, direction).start()
        wcopy(kind, vs, 2).start()

    def swap(i, slot):
        src, dst = (
            (win_a.at[S], win_a.at[slot]),
            (win_b.at[S], win_b.at[slot]),
            (oa_ref, wo.at[slot, pl.ds(0, ow)]),
            (oc_ref, wo.at[slot, pl.ds(ow, cw)]),
            (ext.at[0], ext.at[1]),
            (lse_buf.at[0], lse_buf.at[1]),
        )[i]
        return remote(src, dst, sw_send.at[i], sw_recv.at[i], swp)

    tok_d = remote(tok_ref, tok.at[tp], tok_send.at[0], tok_recv.at[tp], sib)
    tok_y = remote(tok_ref, tok.at[tp], tok_send.at[1], tok_recv.at[tp], (sp, (1 - y) * 2 + x))
    tok_x = remote(tok_ref, tok.at[tp], tok_send.at[2], tok_recv.at[tp], (z * X + 1 - x, y * 2 + x))
    local = [
        pltpu.make_async_copy(tok_ref, tok.at[tp], loc_sem.at[0]),
        pltpu.make_async_copy(oa_ref, wo.at[vs, pl.ds(0, ow)], loc_sem.at[1]),
        pltpu.make_async_copy(oc_ref, wo.at[vs, pl.ds(ow, cw)], loc_sem.at[2]),
    ]

    @pl.when(home)
    def _():
        own_start(0)
        own_start(1)

    @pl.when(foreign)
    def _():
        swap(0, sp).start()

    tok_x.start()
    tok_y.start()

    @pl.when(foreign)
    def _():
        tok_d.start()
        for i in range(1, 5):
            swap(i, sp).start()

    @pl.when(home)
    def _():
        for copy in local:
            copy.start()

    MB = 128
    quarter = HEAD_DIM // 4

    def angles(i, carry):
        r = pl.ds(pl.multiple_of(i * MB, MB), MB)
        pos = vs * rows + i * MB + lax.broadcasted_iota(jnp.int32, (MB, kw), 0)
        lane = lax.broadcasted_iota(jnp.int32, (MB, kw), 1) % HEAD_DIM
        freq = jnp.exp((lane % quarter).astype(jnp.float32) * (-4.0 / HEAD_DIM * math.log(rope_base)))
        index = jnp.where(lane >= 2 * quarter, pos % GRID_W, pos // GRID_W)
        angle = index.astype(jnp.float32) * freq
        cos_ref[r, :] = jnp.cos(angle)
        sin_ref[r, :] = jnp.where(lane % (2 * quarter) < quarter, -1.0, 1.0) * jnp.sin(angle)
        return carry

    def comm(kind, dist):
        for up in (0, 1):
            zz = z + dist * (2 * up - 1)

            @pl.when((zz >= 0) & (zz < Z))
            def _(zz=zz, up=up):
                slot = zz * X + c
                wcopy(kind, slot, 2).wait_recv()

                @pl.when(has_low if up else has_high)
                def _():
                    wcopy(kind, slot, 0 if up else 1).start()
                wcopy(kind, slot, 2).start()

    def relay(cc):
        q = y * 2 + cc
        return remote(tok.at[q], tok.at[q], tok_send.at[3 + cc], tok_recv.at[q], ynb)

    def tok_wait(q):
        remote(tok.at[q], tok.at[q], tok_send.at[0], tok_recv.at[q], ynb).wait_recv()

    RB = 64

    def norm_rows(i, carry):
        r = pl.ds(pl.multiple_of(i * RB, RB), RB)
        total = jnp.zeros((RB, 1), jnp.float32)
        for t in range(TP):
            v = tok[t, r, :].astype(jnp.float32)
            total += jnp.sum(v * v, axis=1, keepdims=True)
        scale = lax.rsqrt(total / (TP * width) + norm_eps)
        for t in range(TP):
            v = tok[t, r, :].astype(jnp.float32)
            g = gain_ref[:, t * width:(t + 1) * width]
            normed[r, t * width:(t + 1) * width] = (v * scale * g).astype(jnp.bfloat16)
        return carry

    PB = 256
    pdepth = X * depth

    def project(kind, zz, first):
        win, acc = ((win_a, acc_a), (win_b, acc_b))[kind]
        n = acc.shape[1]
        wcopy(kind, zz * X + 1 - c, 2).wait_recv()

        def body(i, carry):
            r = pl.ds(pl.multiple_of(i * PB, PB), PB)
            k = pl.ds(pl.multiple_of(zz * pdepth, pdepth), pdepth)
            weight = win[pl.ds(zz * X, X)].reshape(pdepth, n)
            prod = jnp.dot(normed[r, k], weight, preferred_element_type=jnp.float32)
            if first:
                acc[r, :] = prod
            else:
                acc[r, :] += prod
            return carry
        lax.fori_loop(0, rows // PB, body, 0)

    def each_side(dist, fn):
        def step(side, carry):
            zz = z + dist * (2 * side - 1)

            @pl.when((zz >= 0) & (zz < Z))
            def _():
                fn(zz)
            return carry
        lax.fori_loop(0, 2, step, 0)

    def project_at(kind, dist):
        each_side(dist, lambda zz: project(kind, zz, False))

    lax.fori_loop(0, rows // MB, angles, 0)

    @pl.when(foreign)
    def _():
        swap(0, vs).wait_recv()
        own_start(0)

    comm(0, 1)

    @pl.when(foreign)
    def _():
        for cc in range(2):
            tok_wait(y * 2 + cc)
            relay(cc).start()
        swap(1, vs).wait_recv()
        own_start(1)

    comm(1, 1)
    if Z > 2:
        comm(0, 2)

    @pl.when(home)
    def _():
        for copy in local:
            copy.wait()
        tok_wait(y * 2 + 1 - c)
    for cc in range(2):
        tok_wait((1 - y) * 2 + cc)

    lax.fori_loop(0, rows // RB, norm_rows, 0)

    project(0, z, True)
    project(1, z, True)
    project_at(0, 1)
    if Z > 2:
        comm(1, 2)

    @pl.when(foreign)
    def _():
        for i in range(2, 5):
            swap(i, vs).wait_recv()
    own_start(2)
    project_at(1, 1)
    for dist in range(2, Z):
        if dist > 2:
            comm(0, dist)
        project_at(0, dist)

    def turned(v, cosv, sinv):
        lane = lax.broadcasted_iota(jnp.int32, v.shape, 1)
        partner = jnp.where(
            lane % (2 * quarter) < quarter,
            pltpu.roll(v, v.shape[1] - quarter, 1),
            pltpu.roll(v, quarter, 1),
        )
        return v * cosv + partner * sinv

    def k_rows(i, carry):
        r = pl.ds(pl.multiple_of(i * MB, MB), MB)
        v = acc_a[r, qw:qw + kw]
        lane = lax.broadcasted_iota(jnp.int32, v.shape, 1)
        kv = jnp.where(lane < HEAD_DIM, turned(v, cos_ref[r, :], sin_ref[r, :]), v)
        kvp[pl.ds(pl.multiple_of(WINDOW + i * MB, MB), MB), :] = kv.astype(jnp.bfloat16)
        return carry

    lax.fori_loop(0, rows // MB, k_rows, 0)

    def halo(i, src, dst, dev):
        return remote(src, dst, halo_sem.at[2 * i], halo_sem.at[2 * i + 1], dev)

    kv_next = halo(0, kvp.at[pl.ds(rows, WINDOW)], kvp.at[pl.ds(0, WINDOW)], next_dev)
    kv_prev = halo(1, kvp.at[pl.ds(WINDOW, WINDOW)], kvp.at[pl.ds(WINDOW + rows, WINDOW)], prev_dev)
    c_next = halo(2, chalo_out.at[1], chalo_in.at[0], next_dev)
    c_prev = halo(3, chalo_out.at[0], chalo_in.at[1], prev_dev)

    @pl.when(has_next)
    def _():
        kv_next.start()

    @pl.when(has_prev)
    def _():
        kv_prev.start()

    def q_rows(i, carry):
        r = pl.ds(pl.multiple_of(i * MB, MB), MB)
        for k in range(qw // kw):
            qbuf[r, k * kw:(k + 1) * kw] = turned(
                acc_a[r, k * kw:(k + 1) * kw], cos_ref[r, :], sin_ref[r, :]
            ).astype(jnp.bfloat16)
        return carry

    lax.fori_loop(0, rows // MB, q_rows, 0)

    zero_kv = jnp.zeros((WINDOW, kw), jnp.bfloat16)
    zero_c = jnp.zeros((8, cw), jnp.float32)

    @pl.when(has_prev)
    def _():
        kv_next.wait_recv()

    @pl.when(jnp.logical_not(has_prev))
    def _():
        kvp[0:WINDOW, :] = zero_kv

    @pl.when(has_next)
    def _():
        kv_prev.wait_recv()

    @pl.when(jnp.logical_not(has_next))
    def _():
        kvp[WINDOW + rows:, :] = zero_kv

    K3 = 3 * WINDOW
    total_tokens = rows * S

    def attend(b, carry):
        r = pl.ds(pl.multiple_of(b * WINDOW, WINDOW), WINDOW)
        kv = kvp[pl.ds(pl.multiple_of(b * WINDOW, WINDOW), K3), :].astype(jnp.float32)
        lane = lax.broadcasted_iota(jnp.int32, (K3, kw), 1)
        swapped = pltpu.roll(kv, HEAD_DIM, 1)
        kk = jnp.where(lane < HEAD_DIM, kv, swapped).astype(jnp.bfloat16)
        vv = jnp.where(lane < HEAD_DIM, swapped, kv).astype(jnp.bfloat16)
        k_half = [jnp.where(lane < HEAD_DIM, kk, 0), jnp.where(lane < HEAD_DIM, 0, kk)]
        v_half = [jnp.where(lane < HEAD_DIM, vv, 0), jnp.where(lane < HEAD_DIM, 0, vv)]
        qi = lax.broadcasted_iota(jnp.int32, (WINDOW, K3), 0)
        ki = lax.broadcasted_iota(jnp.int32, (WINDOW, K3), 1)
        first = vs * rows + b * WINDOW - WINDOW
        allowed = (ki >= qi) & (ki <= qi + 2 * WINDOW) & (ki + first >= 0) & (ki + first < total_tokens)
        lse_lane = lax.broadcasted_iota(jnp.int32, (WINDOW, WINDOW), 1)
        lse_all = jnp.zeros((WINDOW, WINDOW), jnp.float32)
        for pair in range(heads // 2):
            q = qbuf[r, pair * kw:(pair + 1) * kw]
            total = jnp.zeros((WINDOW, kw), jnp.float32)
            for side in range(2):
                h = pair * 2 + side
                s = lax.dot_general(
                    q, k_half[side], (((1,), (1,)), ((), ())), preferred_element_type=jnp.float32
                ) * HEAD_DIM ** (-0.5)
                s = jnp.where(allowed, s, -jnp.inf)
                sink = ext[role, 3:4, h:h + 1]
                top = jnp.maximum(jnp.max(s, axis=1, keepdims=True), sink)
                e = jnp.exp(s - top)
                den = jnp.sum(e, axis=1, keepdims=True) + jnp.exp(sink - top)
                w = (e * (1.0 / den)).astype(jnp.bfloat16)
                total += jnp.dot(w, v_half[side], preferred_element_type=jnp.float32)
                lse_all = jnp.where(lse_lane == h, top + jnp.log(den), lse_all)
            ac[r, pair * kw:(pair + 1) * kw] = total.astype(jnp.bfloat16)
        lse_buf[0, :, r] = jnp.transpose(lse_all)[0:heads, :]
        return carry

    blocks = rows // WINDOW
    lax.fori_loop(0, blocks, attend, 0)

    @pl.when(foreign)
    def _():
        swap(5, sp).start()

    for dist in range(2, Z):
        if dist > 2:
            comm(1, dist)
        project_at(1, dist)

    def c_rows(i, carry):
        r = pl.ds(pl.multiple_of(i * MB, MB), MB)
        mi = (acc_b[r, cw:2 * cw] * acc_b[r, 2 * cw:3 * cw]).astype(jnp.bfloat16)
        cf[pl.ds(pl.multiple_of(8 + i * MB, 8), MB), :] = mi.astype(jnp.float32)
        return carry

    lax.fori_loop(0, rows // MB, c_rows, 0)
    E = chalo_out.shape[1]
    chalo_out[0] = cf[8:8 + E, :].astype(jnp.bfloat16)
    chalo_out[1] = cf[8 + rows - E:8 + rows, :].astype(jnp.bfloat16)

    @pl.when(has_next)
    def _():
        c_next.start()

    @pl.when(has_prev)
    def _():
        c_prev.start()

    @pl.when(has_prev)
    def _():
        c_next.wait_recv()
        cf[0:8, :] = chalo_in[0, E - 8:E, :].astype(jnp.float32)

    @pl.when(jnp.logical_not(has_prev))
    def _():
        cf[0:8, :] = zero_c

    @pl.when(has_next)
    def _():
        c_prev.wait_recv()
        cf[8 + rows:16 + rows, :] = chalo_in[1, 0:8, :].astype(jnp.float32)

    @pl.when(jnp.logical_not(has_next))
    def _():
        cf[8 + rows:16 + rows, :] = zero_c

    taps = [ext[role, t:t + 1, :] for t in range(3)]
    for i in range(rows // MB):
        a = 8 + i * MB
        conv = (
            taps[0] * cf[a - 1:a - 1 + MB, :]
            + taps[1] * cf[a:a + MB, :]
            + taps[2] * cf[a + 1:a + 1 + MB, :]
        )
        ac[i * MB:(i + 1) * MB, qw:qw + cw] = (acc_b[i * MB:(i + 1) * MB, 0:cw] * conv).astype(jnp.bfloat16)

    mine_dev = (z * X + c, y * 2 + c)
    other_dev = (z * X + c, y * 2 + 1 - c)

    def r1(s, src, dst, dev):
        return remote(send1.at[s, src], recv1.at[s, dst], r1_send.at[s, src], r1_recv.at[s, dst], dev)

    def r2(s, src, dst, dev):
        return remote(send2.at[s, src], recv2.at[s, dst], r2_send.at[s, src], r2_recv.at[s, dst], dev)

    def out_dot(s, yo, m):
        co = c if m == 0 else 1 - c
        r = pl.ds(pl.multiple_of((2 * yo + co) * chunk, chunk), chunk)
        return jnp.dot(ac[r, :], wo[s], preferred_element_type=jnp.float32)

    def produce_x(s):
        for yo in range(2):
            for m in (1, 0):
                v = out_dot(s, yo, m)
                if m == 0:
                    keep[s, yo] = v
                send1[s, m, yo] = v.astype(jnp.bfloat16)
        r1(s, 1, role, other_dev).start()

        @pl.when(foreign)
        def _():
            r1(s, 0, 1, mine_dev).start()

    def produce_y(s):
        for m in range(2):
            send1[s, 0, m] = out_dot(s, 1 - y, m).astype(jnp.bfloat16)
        r1(s, 0, 0, ynb).start()
        for m in range(2):
            keep[s, m] = out_dot(s, y, m)

    def stage_x(s):
        r1(s, 0, 1, mine_dev).wait_recv()

        def pass_on(base):
            send2[s, 0] = (base(1 - y) + recv1[s, 1, 1 - y].astype(jnp.float32)).astype(jnp.bfloat16)
            r2(s, 0, 0, ynb).start()
            keep[s, y] = base(y) + recv1[s, 1, y].astype(jnp.float32)

        @pl.when(home)
        def _():
            pass_on(lambda yo: keep[s, yo])

        @pl.when(foreign)
        def _():
            r1(s, 1, 0, other_dev).wait_recv()
            pass_on(lambda yo: recv1[s, 0, yo].astype(jnp.float32))

    def stage_y(s):
        r1(s, 0, 0, ynb).wait_recv()
        send2[s, 1] = (keep[s, 1] + recv1[s, 0, 1].astype(jnp.float32)).astype(jnp.bfloat16)
        r2(s, 1, role, other_dev).start()
        mine = keep[s, 0] + recv1[s, 0, 0].astype(jnp.float32)

        @pl.when(home)
        def _():
            keep[s, 0] = mine

        @pl.when(foreign)
        def _():
            send2[s, 0] = mine.astype(jnp.bfloat16)
            r2(s, 0, 1, mine_dev).start()

    def place(s, v):
        out_ref[:, pl.ds(pl.multiple_of(s * cols, cols), cols)] = v.astype(jnp.bfloat16)

    def finish_x(s):
        r2(s, 0, 0, ynb).wait_recv()
        place(s, keep[s, y] + recv2[s, 0].astype(jnp.float32))

    def finish_y(s):
        r2(s, 0, 1, mine_dev).wait_recv()
        arrived = recv2[s, 1].astype(jnp.float32)

        @pl.when(home)
        def _():
            place(s, keep[s, 0] + arrived)

        @pl.when(foreign)
        def _():
            r2(s, 1, 0, other_dev).wait_recv()
            place(s, recv2[s, 0].astype(jnp.float32) + arrived)

    def produce(zz):
        wcopy(2, zz * X + 1 - c, 2).wait_recv()
        produce_x(zz * X)
        produce_y(zz * X + 1)

    def stage(zz):
        stage_x(zz * X)
        stage_y(zz * X + 1)

    def finish(zz):
        finish_x(zz * X)
        finish_y(zz * X + 1)

    produce(z)
    for dist in range(1, Z):
        comm(2, dist)
        each_side(dist, produce)
        if dist == 1:
            stage(z)
        else:
            each_side(dist - 1, stage)
    each_side(Z - 1, stage)
    finish(z)
    for dist in range(1, Z):
        each_side(dist, finish)

    @pl.when(home)
    def _():
        lse_ref[...] = lse_buf[0]

    @pl.when(foreign)
    def _():
        swap(5, vs).wait_recv()
        lse_ref[...] = lse_buf[1]
        tok_d.wait_send()
        for cc in range(2):
            relay(cc).wait_send()
        for i in range(6):
            swap(i, sp).wait_send()

    tok_x.wait_send()
    tok_y.wait_send()

    @pl.when(has_next)
    def _():
        kv_next.wait_send()
        c_next.wait_send()

    @pl.when(has_prev)
    def _():
        kv_prev.wait_send()
        c_prev.wait_send()

    def drain(zz, carry):
        slot = zz * X + c
        for kind in range(3):
            for direction, cond in ((0, (zz >= z) & has_low), (1, (zz <= z) & has_high)):
                @pl.when(cond)
                def _(kind=kind, direction=direction):
                    wcopy(kind, slot, direction).wait_send()
            wcopy(kind, slot, 2).wait_send()
        sx, sy = zz * X, zz * X + 1
        r1(sx, 1, role, other_dev).wait_send()
        r1(sy, 0, 0, ynb).wait_send()
        r2(sx, 0, 0, ynb).wait_send()
        r2(sy, 1, role, other_dev).wait_send()

        @pl.when(foreign)
        def _():
            r1(sx, 0, 1, mine_dev).wait_send()
            r2(sy, 0, 1, mine_dev).wait_send()
        return carry

    lax.fori_loop(0, Z, drain, 0)


def fused(
    tokens, norm_gain, w_query, w_key, w_value, w_post_gate, w_pre_gate, w_conv_in,
    conv_taps, sink_logit, w_out_attn, w_out_conv,
):
    S, TP = lax.axis_size("sp"), lax.axis_size("tp")
    X = 2
    Z = S // X
    rows, width = tokens.shape
    depth, qw = w_query.shape
    cw = w_post_gate.shape[1]
    ow, cols = w_out_attn.shape
    heads = qw // HEAD_DIM
    kw = 2 * HEAD_DIM
    chunk = rows // TP
    bf, f32 = jnp.bfloat16, jnp.float32
    dma = pltpu.SemaphoreType.DMA
    return pl.pallas_call(
        functools.partial(fused_kernel, Z, X),
        out_shape=(
            jax.ShapeDtypeStruct((chunk, S * cols), bf),
            jax.ShapeDtypeStruct((heads, rows), f32),
        ),
        in_specs=[pl.BlockSpec(memory_space=pltpu.VMEM)] * 11 + [pl.BlockSpec(memory_space=pltpu.SMEM)],
        out_specs=(pl.BlockSpec(memory_space=pltpu.VMEM),) * 2,
        scratch_shapes=[
            pltpu.VMEM((rows, kw), f32),
            pltpu.VMEM((rows, kw), f32),
            pltpu.VMEM((TP, rows, width), bf),
            pltpu.VMEM((rows, TP * width), bf),
            pltpu.VMEM((S + 1, depth, qw + kw), bf),
            pltpu.VMEM((S + 1, depth, 3 * cw), bf),
            pltpu.VMEM((S, ow + cw, cols), bf),
            pltpu.VMEM((rows, qw + kw), f32),
            pltpu.VMEM((rows, 3 * cw), f32),
            pltpu.VMEM((rows, qw), bf),
            pltpu.VMEM((rows + 2 * WINDOW, kw), bf),
            pltpu.VMEM((rows + 16, cw), f32),
            pltpu.VMEM((2, 16, cw), bf),
            pltpu.VMEM((2, 16, cw), bf),
            pltpu.VMEM((rows, qw + cw), bf),
            pltpu.VMEM((2, 8, cw), f32),
            pltpu.VMEM((2, heads, rows), f32),
            pltpu.VMEM((S, 2, chunk, cols), f32),
            pltpu.VMEM((S, 2, 2, chunk, cols), bf),
            pltpu.VMEM((S, 2, 2, chunk, cols), bf),
            pltpu.VMEM((S, 2, chunk, cols), bf),
            pltpu.VMEM((S, 2, chunk, cols), bf),
            dma((5,)), dma((TP,)),
            dma((3, 3, S)), dma((3, S)),
            dma((6,)), dma((6,)),
            dma((8,)),
            dma((S, 2)), dma((S, 2)), dma((S, 2)), dma((S, 2)),
            dma((3,)),
        ],
        compiler_params=pltpu.CompilerParams(
            collective_id=0, has_side_effects=True, vmem_limit_bytes=60 * 1024 * 1024
        ),
    )(
        tokens, norm_gain[None, :], w_query, w_key.T, w_value.T, w_post_gate, w_pre_gate, w_conv_in,
        w_out_attn, w_out_conv, conv_taps, sink_logit,
    )


def fits(
    tokens, norm_gain, w_query, w_key, w_value, w_post_gate, w_pre_gate, w_conv_in,
    conv_taps, sink_logit, w_out_attn, w_out_conv,
):
    S, TP = lax.axis_size("sp"), lax.axis_size("tp")
    return (
        TP == 4
        and S % 2 == 0
        and S >= 6
        and w_key.shape[1] == HEAD_DIM
        and w_query.shape[0] % 128 == 0
        and w_query.shape[1] % 128 == 0
        and w_post_gate.shape[1] % 128 == 0
        and w_out_attn.shape[1] % 128 == 0
        and tokens.shape[0] % (TP * WINDOW) == 0
        and tokens.shape[1] % 128 == 0
    )


def either(*args):
    return fused(*args) if fits(*args) else on_device(*args)


def solution(mesh):
    placed = (
        P("sp", "tp"),
        P(),
        P("sp", "tp"),
        P("sp", "tp"),
        P("sp", "tp"),
        P("sp", "tp"),
        P("sp", "tp"),
        P("sp", "tp"),
        P(None, "tp"),
        P("tp"),
        P("tp", "sp"),
        P("tp", "sp"),
    )
    return jax.shard_map(
        either,
        mesh=mesh,
        in_specs=placed,
        out_specs=(P(("sp", "tp"), None), P("tp", "sp")),
        check_vma=False,
    )
```

time: 95.7 us -> 91.6 us (0.957)
  the two profiles are of different devices: /device:TPU:16 before, /device:TPU:0 now
where the time goes in v1:
time: 91.6 us; the launch traced here: 91.5 us
  Pallas kernels  88.3 us (96%)
  local copies, waits for them, and re-layouts  2.49 us (3%)
    pallas_call x1, Pallas kernels, fused(): pl.pallas_call(functools.partial(fused_kernel, Z, X), out_shape=(jax.Shap...  88.3 us
    unnamed x4, local copies, waits for them, and re-layouts  2.49 us

profile of v1, /device:TPU:0, one launch (start us, length us, event | category | flops | bytes accessed | tf_op | source)
XLA Modules:
  0.0 91.5 jit_solution(5367273889634721831)
XLA Ops:
  0.6 88.3 %shard_map.131 = (bf16[128,2048]{1,0:T(8,128)(2,1)}, f32[4,512]{1,0:T(4,128)}) custom-call(bf16[512,512]{1,0:T(8,128)(2,1)} %tok_ref.1, f32[1,2048]{1,0:T(1,128)} %bitcast.5, bf16[256,256]{1,0:T(8,128)(2,1)} %wq_ref.1, bf16[64,256]{1,0:T(8,128)(2,1)} %bitcast.3, bf16[64,256]{1,0:T(8,128)(2,1)} %bitcast.4, bf16[256,256]{1,0:T(8,128)(2,1)} %wpost_ref.1, ...), custom_call_target="tpu_custom_call" | custom-call | tf_op jit(solution)/shard_map/pallas_call | solution.py:801
  89.0 0.0 copy-start
  89.0 1.9 %copy.16 = bf16[128,2048]{1,0:T(8,128)(2,1)} copy(bf16[128,2048]{1,0:T(8,128)(2,1)} %get-tuple-element.4) | data formatting | bytes 1048576
  90.9 0.0 copy-done
  90.9 0.6 copy.17
Async XLA Ops:
  89.0 1.9 %copy-start = (f32[4,512]{1,0:T(4,128)S(1)}, f32[4,512]{1,0:T(4,128)}, u32[]{:S(2)}) copy-start(f32[4,512]{1,0:T(4,128)} %get-tuple-element.5) | copy-start | bytes 24580

commit v2 on v1

--- a/solution.py
+++ b/solution.py
@@ -13,6 +13,7 @@
 HEAD_DIM = 64
 WINDOW = 128
 GRID_W = 64
+EDGE = 16
 
 
 rope_base = 10000.0
@@ -201,7 +202,7 @@
     Z, X,
     tok_ref, gain_ref, wq_ref, wk_ref, wv_ref, wpost_ref, wpre_ref, wcin_ref, oa_ref, oc_ref, taps_ref, sink_ref,
     out_ref, lse_ref,
-    cos_ref, sin_ref, tok, normed, win_a, win_b, wo, acc_a, acc_b, qbuf, kvp, cf, chalo_out, chalo_in, ac, ext, lse_buf,
+    cos_ref, sin_ref, tok, normed, win_a, win_b, wo, acc_a, acc_b, qbuf, kvp, cf, ac, ext, lse_buf,
     keep, send1, recv1, send2, recv2,
     tok_send, tok_recv, w_send, w_recv, sw_send, sw_recv, halo_sem, r1_send, r1_recv, r2_send, r2_recv, loc_sem,
 ):
@@ -257,11 +258,8 @@
     heads = qw // HEAD_DIM
     ext[0] = jnp.zeros(ext.shape[1:], jnp.float32)
     ext[0, 0:3, :] = taps_ref[...]
-    ext_lane = lax.broadcasted_iota(jnp.int32, (1, cw), 1)
-    sink_row = jnp.zeros((1, cw), jnp.float32)
     for h in range(heads):
-        sink_row = jnp.where(ext_lane == h, sink_ref[h], sink_row)
-    ext[0, 3:4, :] = sink_row
+        ext[0, 3 + h:4 + h, :] = jnp.full((1, cw), sink_ref[h], jnp.float32)
 
     pl.semaphore_wait(barrier, peers)
 
@@ -296,9 +294,16 @@
         )[i]
         return remote(src, dst, sw_send.at[i], sw_recv.at[i], swp)
 
-    tok_d = remote(tok_ref, tok.at[tp], tok_send.at[0], tok_recv.at[tp], sib)
-    tok_y = remote(tok_ref, tok.at[tp], tok_send.at[1], tok_recv.at[tp], (sp, (1 - y) * 2 + x))
-    tok_x = remote(tok_ref, tok.at[tp], tok_send.at[2], tok_recv.at[tp], (z * X + 1 - x, y * 2 + x))
+    TH = 2
+    part_rows = rows // TH
+
+    def tok_copy(src, q, i, part, dev):
+        r = pl.ds(part * part_rows, part_rows)
+        return remote(src.at[r], tok.at[q, r], tok_send.at[i, part], tok_recv.at[q, part], dev)
+
+    tok_d = [tok_copy(tok_ref, tp, 0, part, sib) for part in range(TH)]
+    tok_y = [tok_copy(tok_ref, tp, 1, part, (sp, (1 - y) * 2 + x)) for part in range(TH)]
+    tok_x = [tok_copy(tok_ref, tp, 2, part, (z * X + 1 - x, y * 2 + x)) for part in range(TH)]
     local = [
         pltpu.make_async_copy(tok_ref, tok.at[tp], loc_sem.at[0]),
         pltpu.make_async_copy(oa_ref, wo.at[vs, pl.ds(0, ow)], loc_sem.at[1]),
@@ -314,13 +319,15 @@
     def _():
         swap(0, sp).start()
 
-    tok_x.start()
-    tok_y.start()
+    for part in range(TH):
+        tok_x[part].start()
+        tok_y[part].start()
 
     @pl.when(foreign)
     def _():
-        tok_d.start()
-        for i in range(1, 5):
+        for copy in tok_d:
+            copy.start()
+        for i in (1, 4, 2, 3):
             swap(i, sp).start()
 
     @pl.when(home)
@@ -342,11 +349,14 @@
         sin_ref[r, :] = jnp.where(lane % (2 * quarter) < quarter, -1.0, 1.0) * jnp.sin(angle)
         return carry
 
-    def comm(kind, dist):
+    def comm(kind, dist, only=None):
         for up in (0, 1):
             zz = z + dist * (2 * up - 1)
-
-            @pl.when((zz >= 0) & (zz < Z))
+            valid = (zz >= 0) & (zz < Z)
+            if only is not None:
+                valid = valid & only
+
+            @pl.when(valid)
             def _(zz=zz, up=up):
                 slot = zz * X + c
                 wcopy(kind, slot, 2).wait_recv()
@@ -356,12 +366,12 @@
                     wcopy(kind, slot, 0 if up else 1).start()
                 wcopy(kind, slot, 2).start()
 
-    def relay(cc):
+    def relay(cc, part):
         q = y * 2 + cc
-        return remote(tok.at[q], tok.at[q], tok_send.at[3 + cc], tok_recv.at[q], ynb)
-
-    def tok_wait(q):
-        remote(tok.at[q], tok.at[q], tok_send.at[0], tok_recv.at[q], ynb).wait_recv()
+        return tok_copy(tok.at[q], q, 3 + cc, part, ynb)
+
+    def tok_wait(q, part):
+        tok_copy(tok.at[q], q, 0, part, ynb).wait_recv()
 
     RB = 64
 
@@ -378,7 +388,6 @@
             normed[r, t * width:(t + 1) * width] = (v * scale * g).astype(jnp.bfloat16)
         return carry
 
-    PB = 256
     pdepth = X * depth
 
     def project(kind, zz, first):
@@ -386,8 +395,10 @@
         n = acc.shape[1]
         wcopy(kind, zz * X + 1 - c, 2).wait_recv()
 
+        pb = acc.shape[0] // 2
+
         def body(i, carry):
-            r = pl.ds(pl.multiple_of(i * PB, PB), PB)
+            r = pl.ds(pl.multiple_of(i * pb, 16), pb)
             k = pl.ds(pl.multiple_of(zz * pdepth, pdepth), pdepth)
             weight = win[pl.ds(zz * X, X)].reshape(pdepth, n)
             prod = jnp.dot(normed[r, k], weight, preferred_element_type=jnp.float32)
@@ -396,7 +407,7 @@
             else:
                 acc[r, :] += prod
             return carry
-        lax.fori_loop(0, rows // PB, body, 0)
+        lax.fori_loop(0, 2, body, 0)
 
     def each_side(dist, fn):
         def step(side, carry):
@@ -411,52 +422,69 @@
     def project_at(kind, dist):
         each_side(dist, lambda zz: project(kind, zz, False))
 
+    def halo(i, src, dst, dev):
+        return remote(src, dst, halo_sem.at[2 * i], halo_sem.at[2 * i + 1], dev)
+
+    kv_next = halo(0, kvp.at[pl.ds(rows, WINDOW)], kvp.at[pl.ds(0, WINDOW)], next_dev)
+    kv_prev = halo(1, kvp.at[pl.ds(WINDOW, WINDOW)], kvp.at[pl.ds(WINDOW + rows, WINDOW)], prev_dev)
+    n_next = halo(2, normed.at[pl.ds(rows - EDGE, EDGE)], normed.at[pl.ds(rows, EDGE)], next_dev)
+    n_prev = halo(3, normed.at[pl.ds(0, EDGE)], normed.at[pl.ds(rows + EDGE, EDGE)], prev_dev)
+
     lax.fori_loop(0, rows // MB, angles, 0)
 
     @pl.when(foreign)
     def _():
         swap(0, vs).wait_recv()
         own_start(0)
+        for cc in range(2):
+            tok_wait(y * 2 + cc, 0)
+            relay(cc, 0).start()
 
     comm(0, 1)
 
     @pl.when(foreign)
     def _():
         for cc in range(2):
-            tok_wait(y * 2 + cc)
-            relay(cc).start()
+            tok_wait(y * 2 + cc, 1)
+            relay(cc, 1).start()
+
+    comm(0, 2)
+
+    @pl.when(foreign)
+    def _():
         swap(1, vs).wait_recv()
         own_start(1)
-
-    comm(1, 1)
-    if Z > 2:
-        comm(0, 2)
+        swap(4, vs).wait_recv()
 
     @pl.when(home)
     def _():
+        comm(1, 1)
         for copy in local:
             copy.wait()
-        tok_wait(y * 2 + 1 - c)
-    for cc in range(2):
-        tok_wait((1 - y) * 2 + cc)
-
-    lax.fori_loop(0, rows // RB, norm_rows, 0)
-
+        for part in range(TH):
+            tok_wait(y * 2 + 1 - c, part)
+    for part in range(TH):
+        for cc in range(2):
+            tok_wait((1 - y) * 2 + cc, part)
+        lax.fori_loop(part * (part_rows // RB), (part + 1) * (part_rows // RB), norm_rows, 0)
+
+    @pl.when(has_next)
+    def _():
+        n_next.start()
+
+    @pl.when(has_prev)
+    def _():
+        n_prev.start()
+
+    for dist in range(3, Z):
+        comm(0, dist)
     project(0, z, True)
-    project(1, z, True)
     project_at(0, 1)
-    if Z > 2:
-        comm(1, 2)
 
     @pl.when(foreign)
     def _():
-        for i in range(2, 5):
-            swap(i, vs).wait_recv()
-    own_start(2)
-    project_at(1, 1)
+        comm(1, 1)
     for dist in range(2, Z):
-        if dist > 2:
-            comm(0, dist)
         project_at(0, dist)
 
     def turned(v, cosv, sinv):
@@ -478,14 +506,6 @@
 
     lax.fori_loop(0, rows // MB, k_rows, 0)
 
-    def halo(i, src, dst, dev):
-        return remote(src, dst, halo_sem.at[2 * i], halo_sem.at[2 * i + 1], dev)
-
-    kv_next = halo(0, kvp.at[pl.ds(rows, WINDOW)], kvp.at[pl.ds(0, WINDOW)], next_dev)
-    kv_prev = halo(1, kvp.at[pl.ds(WINDOW, WINDOW)], kvp.at[pl.ds(WINDOW + rows, WINDOW)], prev_dev)
-    c_next = halo(2, chalo_out.at[1], chalo_in.at[0], next_dev)
-    c_prev = halo(3, chalo_out.at[0], chalo_in.at[1], prev_dev)
-
     @pl.when(has_next)
     def _():
         kv_next.start()
@@ -503,25 +523,6 @@
         return carry
 
     lax.fori_loop(0, rows // MB, q_rows, 0)
-
-    zero_kv = jnp.zeros((WINDOW, kw), jnp.bfloat16)
-    zero_c = jnp.zeros((8, cw), jnp.float32)
-
-    @pl.when(has_prev)
-    def _():
-        kv_next.wait_recv()
-
-    @pl.when(jnp.logical_not(has_prev))
-    def _():
-        kvp[0:WINDOW, :] = zero_kv
-
-    @pl.when(has_next)
-    def _():
-        kv_prev.wait_recv()
-
-    @pl.when(jnp.logical_not(has_next))
-    def _():
-        kvp[WINDOW + rows:, :] = zero_kv
 
     K3 = 3 * WINDOW
     total_tokens = rows * S
@@ -550,11 +551,11 @@
                     q, k_half[side], (((1,), (1,)), ((), ())), preferred_element_type=jnp.float32
                 ) * HEAD_DIM ** (-0.5)
                 s = jnp.where(allowed, s, -jnp.inf)
-                sink = ext[role, 3:4, h:h + 1]
+                sink = ext[role, 3 + h:4 + h, 0:WINDOW]
                 top = jnp.maximum(jnp.max(s, axis=1, keepdims=True), sink)
-                e = jnp.exp(s - top)
+                e = jnp.exp(s - jnp.concatenate([top] * 3, axis=1))
                 den = jnp.sum(e, axis=1, keepdims=True) + jnp.exp(sink - top)
-                w = (e * (1.0 / den)).astype(jnp.bfloat16)
+                w = (e * jnp.concatenate([1.0 / den] * 3, axis=1)).astype(jnp.bfloat16)
                 total += jnp.dot(w, v_half[side], preferred_element_type=jnp.float32)
                 lse_all = jnp.where(lse_lane == h, top + jnp.log(den), lse_all)
             ac[r, pair * kw:(pair + 1) * kw] = total.astype(jnp.bfloat16)
@@ -562,53 +563,95 @@
         return carry
 
     blocks = rows // WINDOW
-    lax.fori_loop(0, blocks, attend, 0)
+    zero_kv = jnp.zeros((WINDOW, kw), jnp.bfloat16)
+
+    def prev_ready():
+        @pl.when(has_prev)
+        def _():
+            kv_next.wait_recv()
+
+        @pl.when(jnp.logical_not(has_prev))
+        def _():
+            kvp[0:WINDOW, :] = zero_kv
+
+    def next_ready():
+        @pl.when(has_next)
+        def _():
+            kv_prev.wait_recv()
+
+        @pl.when(jnp.logical_not(has_next))
+        def _():
+            kvp[WINDOW + rows:, :] = zero_kv
+
+    def edge_ready(at_start):
+        @pl.when(at_start)
+        def _():
+            prev_ready()
+
+        @pl.when(jnp.logical_not(at_start))
+        def _():
+            next_ready()
+
+    def attend_from(i, carry):
+        return attend((1 - c + i) % blocks, carry)
+
+    def b_ready():
+        @pl.when(has_prev)
+        def _():
+            n_next.wait_recv()
+
+        @pl.when(has_next)
+        def _():
+            n_prev.wait_recv()
+
+        @pl.when(jnp.logical_not(has_prev))
+        def _():
+            normed[rows:rows + EDGE, :] = jnp.zeros((EDGE, TP * width), jnp.bfloat16)
+
+        @pl.when(jnp.logical_not(has_next))
+        def _():
+            normed[rows + EDGE:, :] = jnp.zeros((EDGE, TP * width), jnp.bfloat16)
+
+    edge_ready(c == 1)
+    lax.fori_loop(0, blocks // 2, attend_from, 0)
+    b_ready()
+    project(1, z, True)
+    comm(1, 2)
 
     @pl.when(foreign)
     def _():
+        for i in (2, 3):
+            swap(i, vs).wait_recv()
+        own_start(2)
+    lax.fori_loop(blocks // 2, blocks - 1, attend_from, 0)
+    edge_ready(c == 0)
+    lax.fori_loop(blocks - 1, blocks, attend_from, 0)
+
+    @pl.when(foreign)
+    def _():
         swap(5, sp).start()
 
-    for dist in range(2, Z):
-        if dist > 2:
-            comm(1, dist)
+    project_at(1, 1)
+    project_at(1, 2)
+
+    @pl.when(home)
+    def _():
+        own_start(2)
+    for dist in range(3, Z):
+        comm(1, dist)
         project_at(1, dist)
-
-    def c_rows(i, carry):
-        r = pl.ds(pl.multiple_of(i * MB, MB), MB)
-        mi = (acc_b[r, cw:2 * cw] * acc_b[r, 2 * cw:3 * cw]).astype(jnp.bfloat16)
-        cf[pl.ds(pl.multiple_of(8 + i * MB, 8), MB), :] = mi.astype(jnp.float32)
-        return carry
-
-    lax.fori_loop(0, rows // MB, c_rows, 0)
-    E = chalo_out.shape[1]
-    chalo_out[0] = cf[8:8 + E, :].astype(jnp.bfloat16)
-    chalo_out[1] = cf[8 + rows - E:8 + rows, :].astype(jnp.bfloat16)
-
-    @pl.when(has_next)
-    def _():
-        c_next.start()
-
-    @pl.when(has_prev)
-    def _():
-        c_prev.start()
-
-    @pl.when(has_prev)
-    def _():
-        c_next.wait_recv()
-        cf[0:8, :] = chalo_in[0, E - 8:E, :].astype(jnp.float32)
-
-    @pl.when(jnp.logical_not(has_prev))
-    def _():
-        cf[0:8, :] = zero_c
-
-    @pl.when(has_next)
-    def _():
-        c_prev.wait_recv()
-        cf[8 + rows:16 + rows, :] = chalo_in[1, 0:8, :].astype(jnp.float32)
-
-    @pl.when(jnp.logical_not(has_next))
-    def _():
-        cf[8 + rows:16 + rows, :] = zero_c
+    inner = has_low & has_high
+    outer = jnp.logical_not(inner)
+    comm(2, 1, inner)
+
+    def gated(lo, n):
+        return (acc_b[lo:lo + n, cw:2 * cw] * acc_b[lo:lo + n, 2 * cw:3 * cw]).astype(jnp.bfloat16)
+
+    for i in range(rows // MB):
+        cf[8 + i * MB:8 + (i + 1) * MB, :] = gated(i * MB, MB).astype(jnp.float32)
+    edge = gated(rows, 2 * EDGE).astype(jnp.float32)
+    cf[0:8, :] = edge[EDGE - 8:EDGE, :]
+    cf[8 + rows:16 + rows, :] = edge[EDGE:EDGE + 8, :]
 
     taps = [ext[role, t:t + 1, :] for t in range(3)]
     for i in range(rows // MB):
@@ -720,8 +763,9 @@
         finish_y(zz * X + 1)
 
     produce(z)
+    comm(2, 2, inner)
     for dist in range(1, Z):
-        comm(2, dist)
+        comm(2, dist, outer if dist < 3 else None)
         each_side(dist, produce)
         if dist == 1:
             stage(z)
@@ -740,24 +784,26 @@
     def _():
         swap(5, vs).wait_recv()
         lse_ref[...] = lse_buf[1]
-        tok_d.wait_send()
-        for cc in range(2):
-            relay(cc).wait_send()
+        for part in range(TH):
+            tok_d[part].wait_send()
+            for cc in range(2):
+                relay(cc, part).wait_send()
         for i in range(6):
             swap(i, sp).wait_send()
 
-    tok_x.wait_send()
-    tok_y.wait_send()
+    for part in range(TH):
+        tok_x[part].wait_send()
+        tok_y[part].wait_send()
 
     @pl.when(has_next)
     def _():
         kv_next.wait_send()
-        c_next.wait_send()
+        n_next.wait_send()
 
     @pl.when(has_prev)
     def _():
         kv_prev.wait_send()
-        c_prev.wait_send()
+        n_prev.wait_send()
 
     def drain(zz, carry):
         slot = zz * X + c
@@ -810,26 +856,24 @@
             pltpu.VMEM((rows, kw), f32),
             pltpu.VMEM((rows, kw), f32),
             pltpu.VMEM((TP, rows, width), bf),
-            pltpu.VMEM((rows, TP * width), bf),
+            pltpu.VMEM((rows + 2 * EDGE, TP * width), bf),
             pltpu.VMEM((S + 1, depth, qw + kw), bf),
             pltpu.VMEM((S + 1, depth, 3 * cw), bf),
             pltpu.VMEM((S, ow + cw, cols), bf),
             pltpu.VMEM((rows, qw + kw), f32),
-            pltpu.VMEM((rows, 3 * cw), f32),
+            pltpu.VMEM((rows + 2 * EDGE, 3 * cw), f32),
             pltpu.VMEM((rows, qw), bf),
             pltpu.VMEM((rows + 2 * WINDOW, kw), bf),
             pltpu.VMEM((rows + 16, cw), f32),
-            pltpu.VMEM((2, 16, cw), bf),
-            pltpu.VMEM((2, 16, cw), bf),
             pltpu.VMEM((rows, qw + cw), bf),
-            pltpu.VMEM((2, 8, cw), f32),
+            pltpu.VMEM((2, -(-(3 + heads) // 8) * 8, cw), f32),
             pltpu.VMEM((2, heads, rows), f32),
             pltpu.VMEM((S, 2, chunk, cols), f32),
             pltpu.VMEM((S, 2, 2, chunk, cols), bf),
             pltpu.VMEM((S, 2, 2, chunk, cols), bf),
             pltpu.VMEM((S, 2, chunk, cols), bf),
             pltpu.VMEM((S, 2, chunk, cols), bf),
-            dma((5,)), dma((TP,)),
+            dma((5, 2)), dma((TP, 2)),
             dma((3, 3, S)), dma((3, S)),
             dma((6,)), dma((6,)),
             dma((8,)),

time: 91.6 us -> 81.5 us (0.89)
  Pallas kernels: 88.3 us -> 78.2 us
    pallas_call x1, Pallas kernels: 88.3 us -> 78.2 us  [fused(): pl.pallas_call(functools.partial(fused_kernel, Z, X), out_shape=(jax.Shap...]
where the time goes in v2:
time: 81.5 us; the launch traced here: 81.3 us
  Pallas kernels  78.2 us (96%)
  local copies, waits for them, and re-layouts  2.49 us (3%)
    pallas_call x1, Pallas kernels, fused(): pl.pallas_call(functools.partial(fused_kernel, Z, X), out_shape=(jax.Shap...  78.2 us
    unnamed x4, local copies, waits for them, and re-layouts  2.49 us

profile of v2, /device:TPU:0, one launch (start us, length us, event | category | flops | bytes accessed | tf_op | source)
XLA Modules:
  0.0 81.3 jit_solution(18353790255891268634)
XLA Ops:
  0.6 78.2 %shard_map.131 = (bf16[128,2048]{1,0:T(8,128)(2,1)}, f32[4,512]{1,0:T(4,128)}) custom-call(bf16[512,512]{1,0:T(8,128)(2,1)} %tok_ref.1, f32[1,2048]{1,0:T(1,128)} %bitcast.5, bf16[256,256]{1,0:T(8,128)(2,1)} %wq_ref.1, bf16[64,256]{1,0:T(8,128)(2,1)} %bitcast.3, bf16[64,256]{1,0:T(8,128)(2,1)} %bitcast.4, bf16[256,256]{1,0:T(8,128)(2,1)} %wpost_ref.1, ...), custom_call_target="tpu_custom_call" | custom-call | tf_op jit(solution)/shard_map/pallas_call | solution.py:847
  78.8 0.0 copy-start
  78.8 1.9 %copy.16 = bf16[128,2048]{1,0:T(8,128)(2,1)} copy(bf16[128,2048]{1,0:T(8,128)(2,1)} %get-tuple-element.4) | data formatting | bytes 1048576
  80.7 0.0 copy-done
  80.7 0.6 copy.17
Async XLA Ops:
  78.8 1.9 %copy-start = (f32[4,512]{1,0:T(4,128)S(1)}, f32[4,512]{1,0:T(4,128)}, u32[]{:S(2)}) copy-start(f32[4,512]{1,0:T(4,128)} %get-tuple-element.5) | copy-start | bytes 24580

commit v3 on v2

--- a/solution.py
+++ b/solution.py
@@ -204,7 +204,7 @@
     out_ref, lse_ref,
     cos_ref, sin_ref, tok, normed, win_a, win_b, wo, acc_a, acc_b, qbuf, kvp, cf, ac, ext, lse_buf,
     keep, send1, recv1, send2, recv2,
-    tok_send, tok_recv, w_send, w_recv, sw_send, sw_recv, halo_sem, r1_send, r1_recv, r2_send, r2_recv, loc_sem,
+    tok_send, tok_recv, wz_send, wd_send, w_recv, sw_send, sw_recv, halo_sem, r_send, r_recv, loc_sem,
 ):
     S = Z * X
     rows, width = tok_ref.shape
@@ -274,14 +274,29 @@
 
     def wcopy(kind, slot, direction):
         block = bufs[kind].at[slot]
-        return remote(block, block, w_send.at[kind, direction, slot], w_recv.at[kind, slot], targets[direction])
-
-    def own_start(kind):
-        for direction, cond in ((0, has_low), (1, has_high)):
+        ssem = (wz_send, wz_send, wd_send)[direction].at[kind]
+        return remote(block, block, ssem, w_recv.at[kind, slot], targets[direction])
+
+    up_light = 2 * z + 1 < Z
+    inner = has_low & has_high
+    outer = jnp.logical_not(inner)
+
+    def own_far(kind):
+        for direction, cond in ((0, has_low & jnp.logical_not(up_light)), (1, has_high & up_light)):
             @pl.when(cond)
             def _(direction=direction):
                 wcopy(kind, vs, direction).start()
         wcopy(kind, vs, 2).start()
+
+    def own_near(kind):
+        for direction, cond in ((0, has_low & up_light), (1, has_high & jnp.logical_not(up_light))):
+            @pl.when(cond)
+            def _(direction=direction):
+                wcopy(kind, vs, direction).start()
+
+    def own_start(kind):
+        own_near(kind)
+        own_far(kind)
 
     def swap(i, slot):
         src, dst = (
@@ -299,11 +314,11 @@
 
     def tok_copy(src, q, i, part, dev):
         r = pl.ds(part * part_rows, part_rows)
-        return remote(src.at[r], tok.at[q, r], tok_send.at[i, part], tok_recv.at[q, part], dev)
-
-    tok_d = [tok_copy(tok_ref, tp, 0, part, sib) for part in range(TH)]
-    tok_y = [tok_copy(tok_ref, tp, 1, part, (sp, (1 - y) * 2 + x)) for part in range(TH)]
-    tok_x = [tok_copy(tok_ref, tp, 2, part, (z * X + 1 - x, y * 2 + x)) for part in range(TH)]
+        return remote(src.at[r], tok.at[q, r], tok_send.at[i], tok_recv.at[q, part], dev)
+
+    tok_d = [tok_copy(tok_ref, tp, 1, part, sib) for part in range(TH)]
+    tok_y = [tok_copy(tok_ref, tp, 0, part, (sp, (1 - y) * 2 + x)) for part in range(TH)]
+    tok_x = [tok_copy(tok_ref, tp, 0, part, (z * X + 1 - x, y * 2 + x)) for part in range(TH)]
     local = [
         pltpu.make_async_copy(tok_ref, tok.at[tp], loc_sem.at[0]),
         pltpu.make_async_copy(oa_ref, wo.at[vs, pl.ds(0, ow)], loc_sem.at[1]),
@@ -368,7 +383,7 @@
 
     def relay(cc, part):
         q = y * 2 + cc
-        return tok_copy(tok.at[q], q, 3 + cc, part, ynb)
+        return tok_copy(tok.at[q], q, 1, part, ynb)
 
     def tok_wait(q, part):
         tok_copy(tok.at[q], q, 0, part, ynb).wait_recv()
@@ -448,6 +463,9 @@
             tok_wait(y * 2 + cc, 1)
             relay(cc, 1).start()
 
+    @pl.when(home)
+    def _():
+        comm(1, 1)
     comm(0, 2)
 
     @pl.when(foreign)
@@ -458,9 +476,9 @@
 
     @pl.when(home)
     def _():
-        comm(1, 1)
         for copy in local:
             copy.wait()
+        own_far(2)
         for part in range(TH):
             tok_wait(y * 2 + 1 - c, part)
     for part in range(TH):
@@ -476,16 +494,28 @@
     def _():
         n_prev.start()
 
+    @pl.when(foreign)
+    def _():
+        comm(1, 1, inner)
+        for i in (2, 3):
+            swap(i, vs).wait_recv()
+        own_far(2)
+
     for dist in range(3, Z):
         comm(0, dist)
     project(0, z, True)
     project_at(0, 1)
 
-    @pl.when(foreign)
-    def _():
-        comm(1, 1)
+    @pl.when(home)
+    def _():
+        comm(1, 2)
+
     for dist in range(2, Z):
         project_at(0, dist)
+
+    @pl.when(foreign)
+    def _():
+        comm(1, 1, outer)
 
     def turned(v, cosv, sinv):
         lane = lax.broadcasted_iota(jnp.int32, v.shape, 1)
@@ -612,17 +642,24 @@
         def _():
             normed[rows + EDGE:, :] = jnp.zeros((EDGE, TP * width), jnp.bfloat16)
 
+    @pl.when(home)
+    def _():
+        for dist in range(3, Z):
+            comm(1, dist)
+
     edge_ready(c == 1)
     lax.fori_loop(0, blocks // 2, attend_from, 0)
     b_ready()
     project(1, z, True)
-    comm(1, 2)
-
-    @pl.when(foreign)
-    def _():
-        for i in (2, 3):
-            swap(i, vs).wait_recv()
-        own_start(2)
+
+    @pl.when(home)
+    def _():
+        own_near(2)
+
+    @pl.when(foreign)
+    def _():
+        comm(1, 2)
+        own_near(2)
     lax.fori_loop(blocks // 2, blocks - 1, attend_from, 0)
     edge_ready(c == 0)
     lax.fori_loop(blocks - 1, blocks, attend_from, 0)
@@ -634,14 +671,12 @@
     project_at(1, 1)
     project_at(1, 2)
 
-    @pl.when(home)
-    def _():
-        own_start(2)
+    @pl.when(foreign)
+    def _():
+        for dist in range(3, Z):
+            comm(1, dist)
     for dist in range(3, Z):
-        comm(1, dist)
         project_at(1, dist)
-    inner = has_low & has_high
-    outer = jnp.logical_not(inner)
     comm(2, 1, inner)
 
     def gated(lo, n):
@@ -666,11 +701,11 @@
     mine_dev = (z * X + c, y * 2 + c)
     other_dev = (z * X + c, y * 2 + 1 - c)
 
-    def r1(s, src, dst, dev):
-        return remote(send1.at[s, src], recv1.at[s, dst], r1_send.at[s, src], r1_recv.at[s, dst], dev)
-
-    def r2(s, src, dst, dev):
-        return remote(send2.at[s, src], recv2.at[s, dst], r2_send.at[s, src], r2_recv.at[s, dst], dev)
+    def r1(s, src, dst, dev, extra=0):
+        return remote(send1.at[s, src], recv1.at[s, dst], r_send.at[extra], r_recv.at[s, dst], dev)
+
+    def r2(s, src, dst, dev, sem, extra=0):
+        return remote(send2.at[s, src], recv2.at[s, dst], r_send.at[2 + extra], r_recv.at[s, sem], dev)
 
     def out_dot(s, yo, m):
         co = c if m == 0 else 1 - c
@@ -688,7 +723,7 @@
 
         @pl.when(foreign)
         def _():
-            r1(s, 0, 1, mine_dev).start()
+            r1(s, 0, 1, mine_dev, 1).start()
 
     def produce_y(s):
         for m in range(2):
@@ -702,7 +737,7 @@
 
         def pass_on(base):
             send2[s, 0] = (base(1 - y) + recv1[s, 1, 1 - y].astype(jnp.float32)).astype(jnp.bfloat16)
-            r2(s, 0, 0, ynb).start()
+            r2(s, 0, 0, ynb, 2).start()
             keep[s, y] = base(y) + recv1[s, 1, y].astype(jnp.float32)
 
         @pl.when(home)
@@ -717,7 +752,7 @@
     def stage_y(s):
         r1(s, 0, 0, ynb).wait_recv()
         send2[s, 1] = (keep[s, 1] + recv1[s, 0, 1].astype(jnp.float32)).astype(jnp.bfloat16)
-        r2(s, 1, role, other_dev).start()
+        r2(s, 1, role, other_dev, 1 + role).start()
         mine = keep[s, 0] + recv1[s, 0, 0].astype(jnp.float32)
 
         @pl.when(home)
@@ -727,17 +762,17 @@
         @pl.when(foreign)
         def _():
             send2[s, 0] = mine.astype(jnp.bfloat16)
-            r2(s, 0, 1, mine_dev).start()
+            r2(s, 0, 1, mine_dev, 2, 1).start()
 
     def place(s, v):
         out_ref[:, pl.ds(pl.multiple_of(s * cols, cols), cols)] = v.astype(jnp.bfloat16)
 
     def finish_x(s):
-        r2(s, 0, 0, ynb).wait_recv()
+        r2(s, 0, 0, ynb, 2).wait_recv()
         place(s, keep[s, y] + recv2[s, 0].astype(jnp.float32))
 
     def finish_y(s):
-        r2(s, 0, 1, mine_dev).wait_recv()
+        r2(s, 0, 1, mine_dev, 2).wait_recv()
         arrived = recv2[s, 1].astype(jnp.float32)
 
         @pl.when(home)
@@ -746,7 +781,7 @@
 
         @pl.when(foreign)
         def _():
-            r2(s, 1, 0, other_dev).wait_recv()
+            r2(s, 1, 0, other_dev, 1).wait_recv()
             place(s, recv2[s, 0].astype(jnp.float32) + arrived)
 
     def produce(zz):
@@ -763,10 +798,11 @@
         finish_y(zz * X + 1)
 
     produce(z)
-    comm(2, 2, inner)
     for dist in range(1, Z):
         comm(2, dist, outer if dist < 3 else None)
         each_side(dist, produce)
+        if dist == 1:
+            comm(2, 2, inner)
         if dist == 1:
             stage(z)
         else:
@@ -784,17 +820,9 @@
     def _():
         swap(5, vs).wait_recv()
         lse_ref[...] = lse_buf[1]
-        for part in range(TH):
-            tok_d[part].wait_send()
-            for cc in range(2):
-                relay(cc, part).wait_send()
         for i in range(6):
             swap(i, sp).wait_send()
 
-    for part in range(TH):
-        tok_x[part].wait_send()
-        tok_y[part].wait_send()
-
     @pl.when(has_next)
     def _():
         kv_next.wait_send()
@@ -805,27 +833,28 @@
         kv_prev.wait_send()
         n_prev.wait_send()
 
-    def drain(zz, carry):
-        slot = zz * X + c
-        for kind in range(3):
-            for direction, cond in ((0, (zz >= z) & has_low), (1, (zz <= z) & has_high)):
-                @pl.when(cond)
-                def _(kind=kind, direction=direction):
-                    wcopy(kind, slot, direction).wait_send()
-            wcopy(kind, slot, 2).wait_send()
-        sx, sy = zz * X, zz * X + 1
-        r1(sx, 1, role, other_dev).wait_send()
-        r1(sy, 0, 0, ynb).wait_send()
-        r2(sx, 0, 0, ynb).wait_send()
-        r2(sy, 1, role, other_dev).wait_send()
-
-        @pl.when(foreign)
-        def _():
-            r1(sx, 0, 1, mine_dev).wait_send()
-            r2(sy, 0, 1, mine_dev).wait_send()
-        return carry
-
-    lax.fori_loop(0, Z, drain, 0)
+    def sent(block, sem):
+        remote(block, block, sem, sem, sib).wait_send()
+
+    sent(tok.at[pl.ds(0, 2)], tok_send.at[0])
+    for kind in range(3):
+        sent(bufs[kind].at[pl.ds(0, Z)], wd_send.at[kind])
+
+        @pl.when(inner)
+        def _(kind=kind):
+            sent(bufs[kind].at[pl.ds(0, Z + 1)], wz_send.at[kind])
+
+        @pl.when(outer)
+        def _(kind=kind):
+            sent(bufs[kind].at[pl.ds(0, 1)], wz_send.at[kind])
+    sent(send1.at[pl.ds(0, Z)], r_send.at[0])
+    sent(send2.at[pl.ds(0, Z)], r_send.at[2])
+
+    @pl.when(foreign)
+    def _():
+        sent(tok.at[pl.ds(0, 3)], tok_send.at[1])
+        sent(send1.at[pl.ds(0, Z), 0], r_send.at[1])
+        sent(send2.at[pl.ds(0, Z), 0], r_send.at[3])
 
 
 def fused(
@@ -847,8 +876,8 @@
     return pl.pallas_call(
         functools.partial(fused_kernel, Z, X),
         out_shape=(
-            jax.ShapeDtypeStruct((chunk, S * cols), bf),
-            jax.ShapeDtypeStruct((heads, rows), f32),
+            pltpu.VMEM((chunk, S * cols), bf),
+            pltpu.VMEM((heads, rows), f32),
         ),
         in_specs=[pl.BlockSpec(memory_space=pltpu.VMEM)] * 11 + [pl.BlockSpec(memory_space=pltpu.SMEM)],
         out_specs=(pl.BlockSpec(memory_space=pltpu.VMEM),) * 2,
@@ -873,11 +902,11 @@
             pltpu.VMEM((S, 2, 2, chunk, cols), bf),
             pltpu.VMEM((S, 2, chunk, cols), bf),
             pltpu.VMEM((S, 2, chunk, cols), bf),
-            dma((5, 2)), dma((TP, 2)),
-            dma((3, 3, S)), dma((3, S)),
+            dma((2,)), dma((TP, 2)),
+            dma((3,)), dma((3,)), dma((3, S)),
             dma((6,)), dma((6,)),
             dma((8,)),
-            dma((S, 2)), dma((S, 2)), dma((S, 2)), dma((S, 2)),
+            dma((4,)), dma((S, 3)),
             dma((3,)),
         ],
         compiler_params=pltpu.CompilerParams(

time: 81.5 us -> 77.8 us (0.955)
  Pallas kernels: 78.2 us -> 75.7 us
  local copies, waits for them, and re-layouts: 2.49 us -> 1.39 us
    pallas_call x1, Pallas kernels: 78.2 us -> 75.7 us  [fused(): pl.pallas_call(functools.partial(fused_kernel, Z, X), out_shape=(pltpu.VM...]
    unnamed x4 -> x2, local copies, waits for them, and re-layouts: 2.49 us -> 1.39 us
where the time goes in v3:
time: 77.8 us; the launch traced here: 77.7 us
  Pallas kernels  75.7 us (97%)
  local copies, waits for them, and re-layouts  1.39 us (2%)
    pallas_call x1, Pallas kernels, fused(): pl.pallas_call(functools.partial(fused_kernel, Z, X), out_shape=(pltpu.VM...  75.7 us

profile of v3, /device:TPU:0, one launch (start us, length us, event | category | flops | bytes accessed | tf_op | source)
XLA Modules:
  0.0 77.7 jit_solution(4517418274722143333)
XLA Ops:
  0.6 75.7 %shard_map.131 = (bf16[128,2048]{1,0:T(8,128)(2,1)S(1)}, f32[4,512]{1,0:T(4,128)S(1)}) custom-call(bf16[512,512]{1,0:T(8,128)(2,1)} %tok_ref.1, f32[1,2048]{1,0:T(1,128)} %bitcast.5, bf16[256,256]{1,0:T(8,128)(2,1)} %wq_ref.1, bf16[64,256]{1,0:T(8,128)(2,1)} %bitcast.3, bf16[64,256]{1,0:T(8,128)(2,1)} %bitcast.4, bf16[256,256]{1,0:T(8,128)(2,1)} %wpost_ref.1, ...), custom_call_target="tpu_custom_call" | custom-call | tf_op jit(solution)/shard_map/pallas_call | solution.py:876
  76.3 0.8 %copy.16 = bf16[128,2048]{1,0:T(8,128)(2,1)} copy(bf16[128,2048]{1,0:T(8,128)(2,1)S(1)} %get-tuple-element.2) | data formatting | bytes 1048576
  77.1 0.6 copy.17

commit v4 on v3

--- a/solution.py
+++ b/solution.py
@@ -14,6 +14,7 @@
 WINDOW = 128
 GRID_W = 64
 EDGE = 16
+NEAR = 8
 
 
 rope_base = 10000.0
@@ -202,9 +203,9 @@
     Z, X,
     tok_ref, gain_ref, wq_ref, wk_ref, wv_ref, wpost_ref, wpre_ref, wcin_ref, oa_ref, oc_ref, taps_ref, sink_ref,
     out_ref, lse_ref,
-    cos_ref, sin_ref, tok, normed, win_a, win_b, wo, acc_a, acc_b, qbuf, kvp, cf, ac, ext, lse_buf,
-    keep, send1, recv1, send2, recv2,
-    tok_send, tok_recv, wz_send, wd_send, w_recv, sw_send, sw_recv, halo_sem, r_send, r_recv, loc_sem,
+    cos_ref, sin_ref, tok, normed, win_a, win_b, wo, acc_a, acc_b, qbuf, kvp, cf, ac, acg, ext, lse_buf,
+    keep, send1, recv1, send2, recv2, gout, gin,
+    tok_send, tok_recv, wz_send, wd_send, w_recv, sw_send, sw_recv, halo_sem, r_send, r_recv, g_send, g_recv, loc_sem,
 ):
     S = Z * X
     rows, width = tok_ref.shape
@@ -281,6 +282,9 @@
     inner = has_low & has_high
     outer = jnp.logical_not(inner)
 
+    def sent(block, sem):
+        remote(block, block, sem, sem, sib).wait_send()
+
     def own_far(kind):
         for direction, cond in ((0, has_low & jnp.logical_not(up_light)), (1, has_high & up_light)):
             @pl.when(cond)
@@ -364,7 +368,7 @@
         sin_ref[r, :] = jnp.where(lane % (2 * quarter) < quarter, -1.0, 1.0) * jnp.sin(angle)
         return carry
 
-    def comm(kind, dist, only=None):
+    def comm(kind, dist, only=None, forward=True):
         for up in (0, 1):
             zz = z + dist * (2 * up - 1)
             valid = (zz >= 0) & (zz < Z)
@@ -376,9 +380,10 @@
                 slot = zz * X + c
                 wcopy(kind, slot, 2).wait_recv()
 
-                @pl.when(has_low if up else has_high)
-                def _():
-                    wcopy(kind, slot, 0 if up else 1).start()
+                if forward:
+                    @pl.when(has_low if up else has_high)
+                    def _():
+                        wcopy(kind, slot, 0 if up else 1).start()
                 wcopy(kind, slot, 2).start()
 
     def relay(cc, part):
@@ -442,8 +447,8 @@
 
     kv_next = halo(0, kvp.at[pl.ds(rows, WINDOW)], kvp.at[pl.ds(0, WINDOW)], next_dev)
     kv_prev = halo(1, kvp.at[pl.ds(WINDOW, WINDOW)], kvp.at[pl.ds(WINDOW + rows, WINDOW)], prev_dev)
-    n_next = halo(2, normed.at[pl.ds(rows - EDGE, EDGE)], normed.at[pl.ds(rows, EDGE)], next_dev)
-    n_prev = halo(3, normed.at[pl.ds(0, EDGE)], normed.at[pl.ds(rows + EDGE, EDGE)], prev_dev)
+    n_next = halo(2, normed.at[pl.ds(rows - NEAR, NEAR)], normed.at[pl.ds(rows + EDGE - NEAR, NEAR)], next_dev)
+    n_prev = halo(3, normed.at[pl.ds(0, NEAR)], normed.at[pl.ds(rows + EDGE, NEAR)], prev_dev)
 
     lax.fori_loop(0, rows // MB, angles, 0)
 
@@ -556,6 +561,12 @@
 
     K3 = 3 * WINDOW
     total_tokens = rows * S
+
+    guest_dev = (sp + X * jnp.where(inner == up_light, -1, 1), tp)
+    far = jnp.where(up_light, Z - 1, 0)
+
+    def guest_copy(half, r):
+        return remote(ac.at[half, r], acg.at[half, r], g_send.at[half], g_recv.at[half], guest_dev)
 
     def attend(b, carry):
         r = pl.ds(pl.multiple_of(b * WINDOW, WINDOW), WINDOW)
@@ -588,7 +599,11 @@
                 w = (e * jnp.concatenate([1.0 / den] * 3, axis=1)).astype(jnp.bfloat16)
                 total += jnp.dot(w, v_half[side], preferred_element_type=jnp.float32)
                 lse_all = jnp.where(lse_lane == h, top + jnp.log(den), lse_all)
-            ac[r, pair * kw:(pair + 1) * kw] = total.astype(jnp.bfloat16)
+            ac[0, r, pair * kw:(pair + 1) * kw] = total.astype(jnp.bfloat16)
+
+        @pl.when(outer)
+        def _():
+            guest_copy(0, r).start()
         lse_buf[0, :, r] = jnp.transpose(lse_all)[0:heads, :]
         return carry
 
@@ -634,13 +649,17 @@
         def _():
             n_prev.wait_recv()
 
+        zero_n = jnp.zeros((NEAR, TP * width), jnp.bfloat16)
+        normed[rows:rows + EDGE - NEAR, :] = zero_n
+        normed[rows + EDGE + NEAR:, :] = zero_n
+
         @pl.when(jnp.logical_not(has_prev))
         def _():
-            normed[rows:rows + EDGE, :] = jnp.zeros((EDGE, TP * width), jnp.bfloat16)
+            normed[rows + EDGE - NEAR:rows + EDGE, :] = zero_n
 
         @pl.when(jnp.logical_not(has_next))
         def _():
-            normed[rows + EDGE:, :] = jnp.zeros((EDGE, TP * width), jnp.bfloat16)
+            normed[rows + EDGE:rows + EDGE + NEAR, :] = zero_n
 
     @pl.when(home)
     def _():
@@ -651,10 +670,6 @@
     lax.fori_loop(0, blocks // 2, attend_from, 0)
     b_ready()
     project(1, z, True)
-
-    @pl.when(home)
-    def _():
-        own_near(2)
 
     @pl.when(foreign)
     def _():
@@ -670,6 +685,10 @@
 
     project_at(1, 1)
     project_at(1, 2)
+
+    @pl.when(home)
+    def _():
+        own_near(2)
 
     @pl.when(foreign)
     def _():
@@ -696,7 +715,11 @@
             + taps[1] * cf[a:a + MB, :]
             + taps[2] * cf[a + 1:a + 1 + MB, :]
         )
-        ac[i * MB:(i + 1) * MB, qw:qw + cw] = (acc_b[i * MB:(i + 1) * MB, 0:cw] * conv).astype(jnp.bfloat16)
+        ac[1, i * MB:(i + 1) * MB, :] = (acc_b[i * MB:(i + 1) * MB, 0:cw] * conv).astype(jnp.bfloat16)
+
+        @pl.when(outer)
+        def _(i=i):
+            guest_copy(1, pl.ds(i * MB, MB)).start()
 
     mine_dev = (z * X + c, y * 2 + c)
     other_dev = (z * X + c, y * 2 + 1 - c)
@@ -707,15 +730,16 @@
     def r2(s, src, dst, dev, sem, extra=0):
         return remote(send2.at[s, src], recv2.at[s, dst], r_send.at[2 + extra], r_recv.at[s, sem], dev)
 
-    def out_dot(s, yo, m):
+    def out_dot(src, w, yo, m):
         co = c if m == 0 else 1 - c
         r = pl.ds(pl.multiple_of((2 * yo + co) * chunk, chunk), chunk)
-        return jnp.dot(ac[r, :], wo[s], preferred_element_type=jnp.float32)
-
-    def produce_x(s):
+        both = jnp.concatenate([src[0, r, :], src[1, r, :]], axis=1)
+        return jnp.dot(both, wo[w], preferred_element_type=jnp.float32)
+
+    def produce_x(s, w, src):
         for yo in range(2):
             for m in (1, 0):
-                v = out_dot(s, yo, m)
+                v = out_dot(src, w, yo, m)
                 if m == 0:
                     keep[s, yo] = v
                 send1[s, m, yo] = v.astype(jnp.bfloat16)
@@ -725,12 +749,12 @@
         def _():
             r1(s, 0, 1, mine_dev, 1).start()
 
-    def produce_y(s):
+    def produce_y(s, w, src):
         for m in range(2):
-            send1[s, 0, m] = out_dot(s, 1 - y, m).astype(jnp.bfloat16)
+            send1[s, 0, m] = out_dot(src, w, 1 - y, m).astype(jnp.bfloat16)
         r1(s, 0, 0, ynb).start()
         for m in range(2):
-            keep[s, m] = out_dot(s, y, m)
+            keep[s, m] = out_dot(src, w, y, m)
 
     def stage_x(s):
         r1(s, 0, 1, mine_dev).wait_recv()
@@ -767,11 +791,11 @@
     def place(s, v):
         out_ref[:, pl.ds(pl.multiple_of(s * cols, cols), cols)] = v.astype(jnp.bfloat16)
 
-    def finish_x(s):
+    def finish_x(s, place=place):
         r2(s, 0, 0, ynb, 2).wait_recv()
         place(s, keep[s, y] + recv2[s, 0].astype(jnp.float32))
 
-    def finish_y(s):
+    def finish_y(s, place=place):
         r2(s, 0, 1, mine_dev, 2).wait_recv()
         arrived = recv2[s, 1].astype(jnp.float32)
 
@@ -784,10 +808,13 @@
             r2(s, 1, 0, other_dev, 1).wait_recv()
             place(s, recv2[s, 0].astype(jnp.float32) + arrived)
 
+    def produce_from(b, zz, src):
+        produce_x(b, zz * X, src)
+        produce_y(b + 1, zz * X + 1, src)
+
     def produce(zz):
         wcopy(2, zz * X + 1 - c, 2).wait_recv()
-        produce_x(zz * X)
-        produce_y(zz * X + 1)
+        produce_from(zz * X, zz, ac)
 
     def stage(zz):
         stage_x(zz * X)
@@ -797,20 +824,57 @@
         finish_x(zz * X)
         finish_y(zz * X + 1)
 
+    def hand_back(i):
+        return remote(gout.at[i], gin.at[i], g_send.at[2 + i], g_recv.at[2 + i], guest_dev)
+
+    def back(i):
+        def put(s, v):
+            gout[i] = v.astype(jnp.bfloat16)
+            hand_back(i).start()
+        return put
+
     produce(z)
-    for dist in range(1, Z):
-        comm(2, dist, outer if dist < 3 else None)
-        each_side(dist, produce)
-        if dist == 1:
-            comm(2, 2, inner)
-        if dist == 1:
-            stage(z)
-        else:
-            each_side(dist - 1, stage)
-    each_side(Z - 1, stage)
+    comm(2, 1, outer)
+    each_side(1, produce)
+    comm(2, 2, inner, False)
+    stage(z)
+    comm(2, 2, outer, False)
+
+    @pl.when(outer)
+    def _():
+        each_side(2, produce)
+        each_side(1, stage)
+
+    @pl.when(inner)
+    def _():
+        for half in range(2):
+            remote(acg.at[half], acg.at[half], g_send.at[half], g_recv.at[half], guest_dev).wait_recv()
+        wcopy(2, far * X + 1 - c, 2).wait_recv()
+        produce_from(S, far, acg)
+        each_side(1, stage)
+        stage(Z)
+        produce_from(far * X, far, ac)
+    @pl.when(inner)
+    def _():
+        finish_x(S, back(0))
+        finish_y(S + 1, back(1))
+    each_side(2, stage)
     finish(z)
-    for dist in range(1, Z):
-        each_side(dist, finish)
+    each_side(1, finish)
+    each_side(2, finish)
+
+    @pl.when(inner)
+    def _():
+        for i in range(2):
+            hand_back(i).wait_send()
+
+    @pl.when(outer)
+    def _():
+        for i in range(2):
+            hand_back(i).wait_recv()
+            place(far * X + i, gin[i])
+        for half in range(2):
+            sent(ac.at[half], g_send.at[half])
 
     @pl.when(home)
     def _():
@@ -833,28 +897,25 @@
         kv_prev.wait_send()
         n_prev.wait_send()
 
-    def sent(block, sem):
-        remote(block, block, sem, sem, sib).wait_send()
-
     sent(tok.at[pl.ds(0, 2)], tok_send.at[0])
-    for kind in range(3):
-        sent(bufs[kind].at[pl.ds(0, Z)], wd_send.at[kind])
-
-        @pl.when(inner)
-        def _(kind=kind):
-            sent(bufs[kind].at[pl.ds(0, Z + 1)], wz_send.at[kind])
-
-        @pl.when(outer)
-        def _(kind=kind):
-            sent(bufs[kind].at[pl.ds(0, 1)], wz_send.at[kind])
-    sent(send1.at[pl.ds(0, Z)], r_send.at[0])
-    sent(send2.at[pl.ds(0, Z)], r_send.at[2])
+    for cond, pairs, along in ((inner, Z + 1, Z + 1), (outer, Z - 1, 1)):
+        @pl.when(cond)
+        def _(pairs=pairs, along=along):
+            for kind in range(3):
+                fewer = 1 if kind == 2 and along > 1 else 0
+                sent(bufs[kind].at[pl.ds(0, along - fewer)], wz_send.at[kind])
+                sent(bufs[kind].at[pl.ds(0, Z if kind < 2 else min(pairs, Z))], wd_send.at[kind])
+            sent(send1.at[pl.ds(0, pairs)], r_send.at[0])
+            sent(send2.at[pl.ds(0, pairs)], r_send.at[2])
+
+            @pl.when(foreign)
+            def _():
+                sent(send1.at[pl.ds(0, pairs), 0], r_send.at[1])
+                sent(send2.at[pl.ds(0, pairs), 0], r_send.at[3])
 
     @pl.when(foreign)
     def _():
         sent(tok.at[pl.ds(0, 3)], tok_send.at[1])
-        sent(send1.at[pl.ds(0, Z), 0], r_send.at[1])
-        sent(send2.at[pl.ds(0, Z), 0], r_send.at[3])
 
 
 def fused(
@@ -894,19 +955,23 @@
             pltpu.VMEM((rows, qw), bf),
             pltpu.VMEM((rows + 2 * WINDOW, kw), bf),
             pltpu.VMEM((rows + 16, cw), f32),
-            pltpu.VMEM((rows, qw + cw), bf),
+            pltpu.VMEM((2, rows, qw), bf),
+            pltpu.VMEM((2, rows, qw), bf),
             pltpu.VMEM((2, -(-(3 + heads) // 8) * 8, cw), f32),
             pltpu.VMEM((2, heads, rows), f32),
-            pltpu.VMEM((S, 2, chunk, cols), f32),
-            pltpu.VMEM((S, 2, 2, chunk, cols), bf),
-            pltpu.VMEM((S, 2, 2, chunk, cols), bf),
-            pltpu.VMEM((S, 2, chunk, cols), bf),
-            pltpu.VMEM((S, 2, chunk, cols), bf),
+            pltpu.VMEM((S + X, 2, chunk, cols), f32),
+            pltpu.VMEM((S + X, 2, 2, chunk, cols), bf),
+            pltpu.VMEM((S + X, 2, 2, chunk, cols), bf),
+            pltpu.VMEM((S + X, 2, chunk, cols), bf),
+            pltpu.VMEM((S + X, 2, chunk, cols), bf),
+            pltpu.VMEM((X, chunk, cols), bf),
+            pltpu.VMEM((X, chunk, cols), bf),
             dma((2,)), dma((TP, 2)),
             dma((3,)), dma((3,)), dma((3, S)),
             dma((6,)), dma((6,)),
             dma((8,)),
-            dma((4,)), dma((S, 3)),
+            dma((4,)), dma((S + X, 3)),
+            dma((4,)), dma((4,)),
             dma((3,)),
         ],
         compiler_params=pltpu.CompilerParams(
@@ -926,11 +991,11 @@
     return (
         TP == 4
         and S % 2 == 0
-        and S >= 6
+        and S == 8
         and w_key.shape[1] == HEAD_DIM
         and w_query.shape[0] % 128 == 0
         and w_query.shape[1] % 128 == 0
-        and w_post_gate.shape[1] % 128 == 0
+        and w_post_gate.shape[1] == w_query.shape[1]
         and w_out_attn.shape[1] % 128 == 0
         and tokens.shape[0] % (TP * WINDOW) == 0
         and tokens.shape[1] % 128 == 0

time: 77.8 us -> 72.7 us (0.934)
  Pallas kernels: 75.7 us -> 70.2 us
    pallas_call x1, Pallas kernels: 75.7 us -> 70.2 us  [fused(): pl.pallas_call(functools.partial(fused_kernel, Z, X), out_shape=(pltpu.VM...]
where the time goes in v4:
time: 72.7 us; the launch traced here: 72.2 us
  Pallas kernels  70.2 us (97%)
  local copies, waits for them, and re-layouts  1.39 us (2%)
    pallas_call x1, Pallas kernels, fused(): pl.pallas_call(functools.partial(fused_kernel, Z, X), out_shape=(pltpu.VM...  70.2 us

profile of v4, /device:TPU:0, one launch (start us, length us, event | category | flops | bytes accessed | tf_op | source)
XLA Modules:
  0.0 72.2 jit_solution(17960820537616712068)
XLA Ops:
  0.6 70.2 %shard_map.131 = (bf16[128,2048]{1,0:T(8,128)(2,1)S(1)}, f32[4,512]{1,0:T(4,128)S(1)}) custom-call(bf16[512,512]{1,0:T(8,128)(2,1)} %tok_ref.1, f32[1,2048]{1,0:T(1,128)} %bitcast.5, bf16[256,256]{1,0:T(8,128)(2,1)} %wq_ref.1, bf16[64,256]{1,0:T(8,128)(2,1)} %bitcast.3, bf16[64,256]{1,0:T(8,128)(2,1)} %bitcast.4, bf16[256,256]{1,0:T(8,128)(2,1)} %wpost_ref.1, ...), custom_call_target="tpu_custom_call" | custom-call | tf_op jit(solution)/shard_map/pallas_call | solution.py:937
  70.8 0.8 %copy.16 = bf16[128,2048]{1,0:T(8,128)(2,1)} copy(bf16[128,2048]{1,0:T(8,128)(2,1)S(1)} %get-tuple-element.2) | data formatting | bytes 1048576
  71.6 0.6 copy.17

commit v5 on v4

--- a/solution.py
+++ b/solution.py
@@ -214,7 +214,7 @@
     qw = qbuf.shape[1]
     cw = cf.shape[1]
     kw = 2 * HEAD_DIM
-    TP = tok.shape[0]
+    TP = tok.shape[0] - 1
     chunk = rows // TP
     sp = lax.axis_index("sp")
     tp = lax.axis_index("tp")
@@ -251,11 +251,21 @@
         peers = peers + jnp.where(cond, 1, 0)
 
     pslot = jnp.where(home, sp, S)
-    win_a[pslot, :, 0:qw] = wq_ref[...]
+    own_tok = jnp.where(home, tp, TP)
+    load_tok = pltpu.make_async_copy(tok_ref, tok.at[own_tok], loc_sem.at[0])
+    load_a = pltpu.make_async_copy(wq_ref, win_a.at[pslot, :, pl.ds(0, qw)], loc_sem.at[1])
+    load_b = [
+        pltpu.make_async_copy(ref, win_b.at[pslot, :, pl.ds(part * cw, cw)], loc_sem.at[2])
+        for part, ref in enumerate((wpost_ref, wpre_ref, wcin_ref))
+    ]
+    load_c = [
+        pltpu.make_async_copy(ref, wo.at[pslot, pl.ds(part * ow, ow)], loc_sem.at[3])
+        for part, ref in enumerate((oa_ref, oc_ref))
+    ]
+    for copy in (load_a, load_tok, *load_b, *load_c):
+        copy.start()
     kv_t = jnp.concatenate([wk_ref[...], wv_ref[...]], axis=0).astype(jnp.float32)
     win_a[pslot, :, qw:qw + kw] = jnp.transpose(kv_t).astype(jnp.bfloat16)
-    for part, ref in enumerate((wpost_ref, wpre_ref, wcin_ref)):
-        win_b[pslot, :, part * cw:(part + 1) * cw] = ref[...]
     heads = qw // HEAD_DIM
     ext[0] = jnp.zeros(ext.shape[1:], jnp.float32)
     ext[0, 0:3, :] = taps_ref[...]
@@ -279,6 +289,7 @@
         return remote(block, block, ssem, w_recv.at[kind, slot], targets[direction])
 
     up_light = 2 * z + 1 < Z
+    far = jnp.where(up_light, Z - 1, 0)
     inner = has_low & has_high
     outer = jnp.logical_not(inner)
 
@@ -306,8 +317,7 @@
         src, dst = (
             (win_a.at[S], win_a.at[slot]),
             (win_b.at[S], win_b.at[slot]),
-            (oa_ref, wo.at[slot, pl.ds(0, ow)]),
-            (oc_ref, wo.at[slot, pl.ds(ow, cw)]),
+            (wo.at[S], wo.at[slot]),
             (ext.at[0], ext.at[1]),
             (lse_buf.at[0], lse_buf.at[1]),
         )[i]
@@ -320,24 +330,20 @@
         r = pl.ds(part * part_rows, part_rows)
         return remote(src.at[r], tok.at[q, r], tok_send.at[i], tok_recv.at[q, part], dev)
 
-    tok_d = [tok_copy(tok_ref, tp, 1, part, sib) for part in range(TH)]
-    tok_y = [tok_copy(tok_ref, tp, 0, part, (sp, (1 - y) * 2 + x)) for part in range(TH)]
-    tok_x = [tok_copy(tok_ref, tp, 0, part, (z * X + 1 - x, y * 2 + x)) for part in range(TH)]
-    local = [
-        pltpu.make_async_copy(tok_ref, tok.at[tp], loc_sem.at[0]),
-        pltpu.make_async_copy(oa_ref, wo.at[vs, pl.ds(0, ow)], loc_sem.at[1]),
-        pltpu.make_async_copy(oc_ref, wo.at[vs, pl.ds(ow, cw)], loc_sem.at[2]),
-    ]
+    tok_d = [tok_copy(tok.at[own_tok], tp, 1, part, sib) for part in range(TH)]
+    tok_y = [tok_copy(tok.at[own_tok], tp, 0, part, (sp, (1 - y) * 2 + x)) for part in range(TH)]
+    tok_x = [tok_copy(tok.at[own_tok], tp, 0, part, (z * X + 1 - x, y * 2 + x)) for part in range(TH)]
+    load_a.wait()
 
     @pl.when(home)
     def _():
         own_start(0)
-        own_start(1)
 
     @pl.when(foreign)
     def _():
         swap(0, sp).start()
 
+    load_tok.wait()
     for part in range(TH):
         tok_x[part].start()
         tok_y[part].start()
@@ -346,13 +352,21 @@
     def _():
         for copy in tok_d:
             copy.start()
-        for i in (1, 4, 2, 3):
+
+    def loaded(block, sem):
+        pltpu.make_async_copy(block, block, sem).wait()
+
+    loaded(win_b.at[pslot], loc_sem.at[2])
+    loaded(wo.at[pslot], loc_sem.at[3])
+
+    @pl.when(home)
+    def _():
+        own_start(1)
+
+    @pl.when(foreign)
+    def _():
+        for i in (1, 3, 2):
             swap(i, sp).start()
-
-    @pl.when(home)
-    def _():
-        for copy in local:
-            copy.start()
 
     MB = 128
     quarter = HEAD_DIM // 4
@@ -410,19 +424,20 @@
 
     pdepth = X * depth
 
-    def project(kind, zz, first):
+    def project(kind, first, planes, fresh):
         win, acc = ((win_a, acc_a), (win_b, acc_b))[kind]
         n = acc.shape[1]
-        wcopy(kind, zz * X + 1 - c, 2).wait_recv()
-
+        kk = planes * pdepth
+        for p in range(planes):
+            wcopy(kind, (first + p) * X + 1 - c, 2).wait_recv()
         pb = acc.shape[0] // 2
 
         def body(i, carry):
             r = pl.ds(pl.multiple_of(i * pb, 16), pb)
-            k = pl.ds(pl.multiple_of(zz * pdepth, pdepth), pdepth)
-            weight = win[pl.ds(zz * X, X)].reshape(pdepth, n)
+            k = pl.ds(pl.multiple_of(first * pdepth, pdepth), kk)
+            weight = win[pl.ds(first * X, planes * X)].reshape(kk, n)
             prod = jnp.dot(normed[r, k], weight, preferred_element_type=jnp.float32)
-            if first:
+            if fresh:
                 acc[r, :] = prod
             else:
                 acc[r, :] += prod
@@ -439,9 +454,6 @@
             return carry
         lax.fori_loop(0, 2, step, 0)
 
-    def project_at(kind, dist):
-        each_side(dist, lambda zz: project(kind, zz, False))
-
     def halo(i, src, dst, dev):
         return remote(src, dst, halo_sem.at[2 * i], halo_sem.at[2 * i + 1], dev)
 
@@ -456,7 +468,7 @@
     def _():
         swap(0, vs).wait_recv()
         own_start(0)
-        for cc in range(2):
+        for cc in (c, 1 - c):
             tok_wait(y * 2 + cc, 0)
             relay(cc, 0).start()
 
@@ -464,7 +476,7 @@
 
     @pl.when(foreign)
     def _():
-        for cc in range(2):
+        for cc in (c, 1 - c):
             tok_wait(y * 2 + cc, 1)
             relay(cc, 1).start()
 
@@ -477,16 +489,17 @@
     def _():
         swap(1, vs).wait_recv()
         own_start(1)
-        swap(4, vs).wait_recv()
+        swap(3, vs).wait_recv()
 
     @pl.when(home)
     def _():
-        for copy in local:
-            copy.wait()
         own_far(2)
         for part in range(TH):
             tok_wait(y * 2 + 1 - c, part)
     for part in range(TH):
+        if part == TH - 1:
+            for dist in range(3, Z):
+                comm(0, dist)
         for cc in range(2):
             tok_wait((1 - y) * 2 + cc, part)
         lax.fori_loop(part * (part_rows // RB), (part + 1) * (part_rows // RB), norm_rows, 0)
@@ -499,27 +512,17 @@
     def _():
         n_prev.start()
 
+    @pl.when(home)
+    def _():
+        comm(1, 2)
+
+    project(0, jnp.int32(0), Z, True)
+
     @pl.when(foreign)
     def _():
         comm(1, 1, inner)
-        for i in (2, 3):
-            swap(i, vs).wait_recv()
+        swap(2, vs).wait_recv()
         own_far(2)
-
-    for dist in range(3, Z):
-        comm(0, dist)
-    project(0, z, True)
-    project_at(0, 1)
-
-    @pl.when(home)
-    def _():
-        comm(1, 2)
-
-    for dist in range(2, Z):
-        project_at(0, dist)
-
-    @pl.when(foreign)
-    def _():
         comm(1, 1, outer)
 
     def turned(v, cosv, sinv):
@@ -563,7 +566,6 @@
     total_tokens = rows * S
 
     guest_dev = (sp + X * jnp.where(inner == up_light, -1, 1), tp)
-    far = jnp.where(up_light, Z - 1, 0)
 
     def guest_copy(half, r):
         return remote(ac.at[half, r], acg.at[half, r], g_send.at[half], g_recv.at[half], guest_dev)
@@ -638,7 +640,9 @@
             next_ready()
 
     def attend_from(i, carry):
-        return attend((1 - c + i) % blocks, carry)
+        near = jnp.where(c == 0, blocks - 1, 0)
+        edge_block = jnp.where(i == blocks - 2, near, blocks - 1 - near)
+        return attend(jnp.where(i < blocks - 2, i + 1, edge_block), carry)
 
     def b_ready():
         @pl.when(has_prev)
@@ -666,25 +670,23 @@
         for dist in range(3, Z):
             comm(1, dist)
 
+    lax.fori_loop(0, blocks - 2, attend_from, 0)
     edge_ready(c == 1)
-    lax.fori_loop(0, blocks // 2, attend_from, 0)
     b_ready()
-    project(1, z, True)
 
     @pl.when(foreign)
     def _():
         comm(1, 2)
         own_near(2)
-    lax.fori_loop(blocks // 2, blocks - 1, attend_from, 0)
+    lax.fori_loop(blocks - 2, blocks - 1, attend_from, 0)
     edge_ready(c == 0)
     lax.fori_loop(blocks - 1, blocks, attend_from, 0)
 
     @pl.when(foreign)
     def _():
-        swap(5, sp).start()
-
-    project_at(1, 1)
-    project_at(1, 2)
+        swap(4, sp).start()
+
+    project(1, jnp.where(up_light, 0, 1), Z - 1, True)
 
     @pl.when(home)
     def _():
@@ -694,8 +696,7 @@
     def _():
         for dist in range(3, Z):
             comm(1, dist)
-    for dist in range(3, Z):
-        project_at(1, dist)
+    project(1, far, 1, False)
     comm(2, 1, inner)
 
     def gated(lo, n):
@@ -737,13 +738,14 @@
         return jnp.dot(both, wo[w], preferred_element_type=jnp.float32)
 
     def produce_x(s, w, src):
-        for yo in range(2):
-            for m in (1, 0):
+        for m in (1, 0):
+            for yo in range(2):
                 v = out_dot(src, w, yo, m)
                 if m == 0:
                     keep[s, yo] = v
                 send1[s, m, yo] = v.astype(jnp.bfloat16)
-        r1(s, 1, role, other_dev).start()
+            if m == 1:
+                r1(s, 1, role, other_dev).start()
 
         @pl.when(foreign)
         def _():
@@ -813,8 +815,20 @@
         produce_y(b + 1, zz * X + 1, src)
 
     def produce(zz):
-        wcopy(2, zz * X + 1 - c, 2).wait_recv()
-        produce_from(zz * X, zz, ac)
+        def sibling_ready():
+            wcopy(2, zz * X + 1 - c, 2).wait_recv()
+
+        @pl.when(c == 0)
+        def _():
+            produce_x(zz * X, zz * X, ac)
+            sibling_ready()
+            produce_y(zz * X + 1, zz * X + 1, ac)
+
+        @pl.when(c == 1)
+        def _():
+            produce_y(zz * X + 1, zz * X + 1, ac)
+            sibling_ready()
+            produce_x(zz * X, zz * X, ac)
 
     def stage(zz):
         stage_x(zz * X)
@@ -882,9 +896,9 @@
 
     @pl.when(foreign)
     def _():
-        swap(5, vs).wait_recv()
+        swap(4, vs).wait_recv()
         lse_ref[...] = lse_buf[1]
-        for i in range(6):
+        for i in range(5):
             swap(i, sp).wait_send()
 
     @pl.when(has_next)
@@ -940,16 +954,19 @@
             pltpu.VMEM((chunk, S * cols), bf),
             pltpu.VMEM((heads, rows), f32),
         ),
-        in_specs=[pl.BlockSpec(memory_space=pltpu.VMEM)] * 11 + [pl.BlockSpec(memory_space=pltpu.SMEM)],
+        in_specs=[
+            pl.BlockSpec(memory_space=space)
+            for space in (pl.ANY, pltpu.VMEM, pl.ANY, *[pltpu.VMEM] * 2, *[pl.ANY] * 5, pltpu.VMEM, pltpu.SMEM)
+        ],
         out_specs=(pl.BlockSpec(memory_space=pltpu.VMEM),) * 2,
         scratch_shapes=[
             pltpu.VMEM((rows, kw), f32),
             pltpu.VMEM((rows, kw), f32),
-            pltpu.VMEM((TP, rows, width), bf),
+            pltpu.VMEM((TP + 1, rows, width), bf),
             pltpu.VMEM((rows + 2 * EDGE, TP * width), bf),
             pltpu.VMEM((S + 1, depth, qw + kw), bf),
             pltpu.VMEM((S + 1, depth, 3 * cw), bf),
-            pltpu.VMEM((S, ow + cw, cols), bf),
+            pltpu.VMEM((S + 1, ow + cw, cols), bf),
             pltpu.VMEM((rows, qw + kw), f32),
             pltpu.VMEM((rows + 2 * EDGE, 3 * cw), f32),
             pltpu.VMEM((rows, qw), bf),
@@ -968,11 +985,11 @@
             pltpu.VMEM((X, chunk, cols), bf),
             dma((2,)), dma((TP, 2)),
             dma((3,)), dma((3,)), dma((3, S)),
-            dma((6,)), dma((6,)),
+            dma((5,)), dma((5,)),
             dma((8,)),
             dma((4,)), dma((S + X, 3)),
             dma((4,)), dma((4,)),
-            dma((3,)),
+            dma((4,)),
         ],
         compiler_params=pltpu.CompilerParams(
             collective_id=0, has_side_effects=True, vmem_limit_bytes=60 * 1024 * 1024

time: 72.7 us -> 72.4 us (level); the launches traced: 72.2 us -> 71 us
  Pallas kernels: 70.2 us -> 69 us
    pallas_call x1, Pallas kernels: 70.2 us -> 69 us  [fused(): pl.pallas_call(functools.partial(fused_kernel, Z, X), out_shape=(pltpu.VM...]
where the time goes in v5:
time: 72.4 us; the launch traced here: 71 us
  Pallas kernels  69 us (95%)
  local copies, waits for them, and re-layouts  1.39 us (2%)
    pallas_call x1, Pallas kernels, fused(): pl.pallas_call(functools.partial(fused_kernel, Z, X), out_shape=(pltpu.VM...  69 us

profile of v5, /device:TPU:0, one launch (start us, length us, event | category | flops | bytes accessed | tf_op | source)
XLA Modules:
  0.0 71.0 jit_solution(7290372432868579406)
XLA Ops:
  0.6 69.0 %shard_map.131 = (bf16[128,2048]{1,0:T(8,128)(2,1)S(1)}, f32[4,512]{1,0:T(4,128)S(1)}) custom-call(bf16[512,512]{1,0:T(8,128)(2,1)} %tok_ref.1, f32[1,2048]{1,0:T(1,128)} %bitcast.5, bf16[256,256]{1,0:T(8,128)(2,1)} %wq_ref.1, bf16[64,256]{1,0:T(8,128)(2,1)} %bitcast.3, bf16[64,256]{1,0:T(8,128)(2,1)} %bitcast.4, bf16[256,256]{1,0:T(8,128)(2,1)} %wpost_ref.1, ...), custom_call_target="tpu_custom_call" | custom-call | tf_op jit(solution)/shard_map/pallas_call | solution.py:951
  69.6 0.8 %copy.16 = bf16[128,2048]{1,0:T(8,128)(2,1)} copy(bf16[128,2048]{1,0:T(8,128)(2,1)S(1)} %get-tuple-element.2) | data formatting | bytes 1048576
  70.4 0.6 copy.17

commit v6 on v5

--- a/solution.py
+++ b/solution.py
@@ -688,15 +688,15 @@
 
     project(1, jnp.where(up_light, 0, 1), Z - 1, True)
 
-    @pl.when(home)
-    def _():
-        own_near(2)
-
     @pl.when(foreign)
     def _():
         for dist in range(3, Z):
             comm(1, dist)
     project(1, far, 1, False)
+    @pl.when(home)
+    def _():
+        own_near(2)
+
     comm(2, 1, inner)
 
     def gated(lo, n):
@@ -731,32 +731,32 @@
     def r2(s, src, dst, dev, sem, extra=0):
         return remote(send2.at[s, src], recv2.at[s, dst], r_send.at[2 + extra], r_recv.at[s, sem], dev)
 
-    def out_dot(src, w, yo, m):
-        co = c if m == 0 else 1 - c
-        r = pl.ds(pl.multiple_of((2 * yo + co) * chunk, chunk), chunk)
+    def out_dot(src, w, yo):
+        r = pl.ds(pl.multiple_of(yo * 2 * chunk, chunk), 2 * chunk)
         both = jnp.concatenate([src[0, r, :], src[1, r, :]], axis=1)
-        return jnp.dot(both, wo[w], preferred_element_type=jnp.float32)
-
-    def produce_x(s, w, src):
-        for m in (1, 0):
-            for yo in range(2):
-                v = out_dot(src, w, yo, m)
-                if m == 0:
-                    keep[s, yo] = v
-                send1[s, m, yo] = v.astype(jnp.bfloat16)
-            if m == 1:
-                r1(s, 1, role, other_dev).start()
+        v = jnp.dot(both, wo[w], preferred_element_type=jnp.float32)
+        return v[0:chunk], v[chunk:2 * chunk]
+
+    def produce_x(s, w, src, core):
+        for yo in range(2):
+            v = out_dot(src, w, yo)
+            keep[s, yo] = v[core]
+            send1[s, 0, yo] = v[core].astype(jnp.bfloat16)
+            send1[s, 1, yo] = v[1 - core].astype(jnp.bfloat16)
+        r1(s, 1, role, other_dev).start()
 
         @pl.when(foreign)
         def _():
             r1(s, 0, 1, mine_dev, 1).start()
 
-    def produce_y(s, w, src):
-        for m in range(2):
-            send1[s, 0, m] = out_dot(src, w, 1 - y, m).astype(jnp.bfloat16)
+    def produce_y(s, w, src, core):
+        v = out_dot(src, w, 1 - y)
+        send1[s, 0, 0] = v[core].astype(jnp.bfloat16)
+        send1[s, 0, 1] = v[1 - core].astype(jnp.bfloat16)
         r1(s, 0, 0, ynb).start()
-        for m in range(2):
-            keep[s, m] = out_dot(src, w, y, m)
+        v = out_dot(src, w, y)
+        keep[s, 0] = v[core]
+        keep[s, 1] = v[1 - core]
 
     def stage_x(s):
         r1(s, 0, 1, mine_dev).wait_recv()
@@ -810,25 +810,21 @@
             r2(s, 1, 0, other_dev, 1).wait_recv()
             place(s, recv2[s, 0].astype(jnp.float32) + arrived)
 
-    def produce_from(b, zz, src):
-        produce_x(b, zz * X, src)
-        produce_y(b + 1, zz * X + 1, src)
+    def produce_from(b, zz, src, sibling_ready=lambda: None):
+        @pl.when(c == 0)
+        def _():
+            produce_x(b, zz * X, src, 0)
+            sibling_ready()
+            produce_y(b + 1, zz * X + 1, src, 0)
+
+        @pl.when(c == 1)
+        def _():
+            produce_y(b + 1, zz * X + 1, src, 1)
+            sibling_ready()
+            produce_x(b, zz * X, src, 1)
 
     def produce(zz):
-        def sibling_ready():
-            wcopy(2, zz * X + 1 - c, 2).wait_recv()
-
-        @pl.when(c == 0)
-        def _():
-            produce_x(zz * X, zz * X, ac)
-            sibling_ready()
-            produce_y(zz * X + 1, zz * X + 1, ac)
-
-        @pl.when(c == 1)
-        def _():
-            produce_y(zz * X + 1, zz * X + 1, ac)
-            sibling_ready()
-            produce_x(zz * X, zz * X, ac)
+        produce_from(zz * X, zz, ac, lambda: wcopy(2, zz * X + 1 - c, 2).wait_recv())
 
     def stage(zz):
         stage_x(zz * X)
@@ -948,7 +944,7 @@
     chunk = rows // TP
     bf, f32 = jnp.bfloat16, jnp.float32
     dma = pltpu.SemaphoreType.DMA
-    return pl.pallas_call(
+    mixed, log_sum = pl.pallas_call(
         functools.partial(fused_kernel, Z, X),
         out_shape=(
             pltpu.VMEM((chunk, S * cols), bf),
@@ -998,6 +994,24 @@
         tokens, norm_gain[None, :], w_query, w_key.T, w_value.T, w_post_gate, w_pre_gate, w_conv_in,
         w_out_attn, w_out_conv, conv_taps, sink_logit,
     )
+    return pl.pallas_call(
+        store_kernel,
+        out_shape=(jax.ShapeDtypeStruct(mixed.shape, bf), jax.ShapeDtypeStruct(log_sum.shape, f32)),
+        in_specs=[pl.BlockSpec(memory_space=pltpu.VMEM)] * 2,
+        out_specs=(pl.BlockSpec(memory_space=pl.ANY),) * 2,
+        scratch_shapes=[dma((2,))],
+    )(*(pltpu.with_memory_space_constraint(v, pltpu.VMEM) for v in (mixed, log_sum)))
+
+
+def store_kernel(mixed_ref, log_sum_ref, out_ref, lse_ref, sem):
+    copies = [
+        pltpu.make_async_copy(src, dst, sem.at[i])
+        for i, (src, dst) in enumerate(((log_sum_ref, lse_ref), (mixed_ref, out_ref)))
+    ]
+    for copy in copies:
+        copy.start()
+    for copy in copies:
+        copy.wait()
 
 
 def fits(

time: 72.4 us -> 71.9 us (level)
  the two profiles are of different devices: /device:TPU:0 before, /device:TPU:8 now
where the time goes in v6:
time: 71.9 us; the launch traced here: 71.7 us
  Pallas kernels  71.1 us (99%)
    pallas_call x1, Pallas kernels, fused(): pl.pallas_call(functools.partial(fused_kernel, Z, X), out_shape=(pltpu.VM...  70.3 us

profile of v6, /device:TPU:8, one launch (start us, length us, event | category | flops | bytes accessed | tf_op | source)
XLA Modules:
  0.0 71.7 jit_solution(6094373110293257737)
XLA Ops:
  0.6 70.3 %shard_map.131 = (bf16[128,2048]{1,0:T(8,128)(2,1)S(1)}, f32[4,512]{1,0:T(4,128)S(1)}) custom-call(bf16[512,512]{1,0:T(8,128)(2,1)} %tok_ref.1, f32[1,2048]{1,0:T(1,128)} %bitcast.5, bf16[256,256]{1,0:T(8,128)(2,1)} %wq_ref.1, bf16[64,256]{1,0:T(8,128)(2,1)} %bitcast.3, bf16[64,256]{1,0:T(8,128)(2,1)} %bitcast.4, bf16[256,256]{1,0:T(8,128)(2,1)} %wpost_ref.1, ...), custom_call_target="tpu_custom_call" | custom-call | tf_op jit(solution)/shard_map/pallas_call | solution.py:947
  70.9 0.8 %shard_map.132 = (bf16[128,2048]{1,0:T(8,128)(2,1)}, f32[4,512]{1,0:T(4,128)}) custom-call(bf16[128,2048]{1,0:T(8,128)(2,1)S(1)} %get-tuple-element.4.mixed_ref, f32[4,512]{1,0:T(4,128)S(1)} %get-tuple-element.5.log_sum_ref), custom_call_target="tpu_custom_call" | custom-call | tf_op jit(solution)/shard_map/pallas_call | solution.py:997

commit v7 on v6

--- a/solution.py
+++ b/solution.py
@@ -430,10 +430,10 @@
         kk = planes * pdepth
         for p in range(planes):
             wcopy(kind, (first + p) * X + 1 - c, 2).wait_recv()
-        pb = acc.shape[0] // 2
+        pb = acc.shape[0]
 
         def body(i, carry):
-            r = pl.ds(pl.multiple_of(i * pb, 16), pb)
+            r = pl.ds(0, pb)
             k = pl.ds(pl.multiple_of(first * pdepth, pdepth), kk)
             weight = win[pl.ds(first * X, planes * X)].reshape(kk, n)
             prod = jnp.dot(normed[r, k], weight, preferred_element_type=jnp.float32)
@@ -442,7 +442,7 @@
             else:
                 acc[r, :] += prod
             return carry
-        lax.fori_loop(0, 2, body, 0)
+        body(0, 0)
 
     def each_side(dist, fn):
         def step(side, carry):
@@ -862,12 +862,13 @@
         wcopy(2, far * X + 1 - c, 2).wait_recv()
         produce_from(S, far, acg)
         each_side(1, stage)
-        stage(Z)
+        stage_y(S + 1)
+        stage_x(S)
         produce_from(far * X, far, ac)
     @pl.when(inner)
     def _():
+        finish_y(S + 1, back(1))
         finish_x(S, back(0))
-        finish_y(S + 1, back(1))
     each_side(2, stage)
     finish(z)
     each_side(1, finish)

time: 71.9 us -> 71.9 us (level)
  the two profiles are of different devices: /device:TPU:8 before, /device:TPU:0 now
where the time goes in v7:
time: 71.9 us; the launch traced here: 70.8 us
  Pallas kernels  70.1 us (97%)
    pallas_call x1, Pallas kernels, fused(): pl.pallas_call(functools.partial(fused_kernel, Z, X), out_shape=(pltpu.VM...  69.3 us

profile of v7, /device:TPU:0, one launch (start us, length us, event | category | flops | bytes accessed | tf_op | source)
XLA Modules:
  0.0 70.8 jit_solution(1692398852996104323)
XLA Ops:
  0.6 69.3 %shard_map.131 = (bf16[128,2048]{1,0:T(8,128)(2,1)S(1)}, f32[4,512]{1,0:T(4,128)S(1)}) custom-call(bf16[512,512]{1,0:T(8,128)(2,1)} %tok_ref.1, f32[1,2048]{1,0:T(1,128)} %bitcast.5, bf16[256,256]{1,0:T(8,128)(2,1)} %wq_ref.1, bf16[64,256]{1,0:T(8,128)(2,1)} %bitcast.3, bf16[64,256]{1,0:T(8,128)(2,1)} %bitcast.4, bf16[256,256]{1,0:T(8,128)(2,1)} %wpost_ref.1, ...), custom_call_target="tpu_custom_call" | custom-call | tf_op jit(solution)/shard_map/pallas_call | solution.py:948
  70.0 0.8 %shard_map.132 = (bf16[128,2048]{1,0:T(8,128)(2,1)}, f32[4,512]{1,0:T(4,128)}) custom-call(bf16[128,2048]{1,0:T(8,128)(2,1)S(1)} %get-tuple-element.4.mixed_ref, f32[4,512]{1,0:T(4,128)S(1)} %get-tuple-element.5.log_sum_ref), custom_call_target="tpu_custom_call" | custom-call | tf_op jit(solution)/shard_map/pallas_call | solution.py:998
